TPU v7x, 32 devices: a whole 2x2x4 slice. The times are simulated.
32 devices in a mesh: sp: 8 (over z, x), tp: 4 (over y, core).
Axes of the slice: x: 2, y: 2, z: 4, core: 2. Of those that a mesh axis runs over, the one named last changes fastest.
Arguments:
- tokens: bfloat16 [2048, 2048], P(('sp', 'tp')), may hold values from -40 to 40
- w_query: bfloat16 [2048, 1024], P(None, 'tp'), may hold values from -0.125 to 0.125
- w_key: bfloat16 [2048, 256], P(None, 'tp'), may hold values from -0.125 to 0.125
- w_value: bfloat16 [2048, 256], P(None, 'tp'), may hold values from -0.125 to 0.125
- w_out: bfloat16 [1024, 2048], P('tp'), may hold values from -0.1875 to 0.1875
- cum_gate: float32 [16, 2048], P('tp', 'sp'), may hold values from -295 to 0, as said below
Outputs:
- layer_out: bfloat16 [2048, 2048], P(('sp', 'tp'))
Inputs may be any that keep to these rules, and one draw needn't show every extreme that they name: `cum_gate`: each head's row does not rise along the positions.
All inputs are finite; a program needn't handle non-finite values.
Results may differ from a plain program's by a relative error of at most 0.012.
Values may be sent and summed in bfloat16 or wider, within the bound.
A program may use at most 64 MiB of HBM per device.

v0:
```python
import functools

import jax
import jax.numpy as jnp
from jax import lax
from jax.experimental import pallas as pl
from jax.experimental.pallas import tpu as pltpu
from jax.sharding import PartitionSpec as P

HD = 64
MESH = pl.DeviceIdType.MESH
CHUNKS = 4


def kernel(
    sp_size, tok, wq, wk, wv, wo, gate, out,
    x, wqv, wboth, wov, gv, kv, qt, top, tot, acc, att, pf, own,
    s_near, s_far, s_own, r_near, r_far, r_own,
    load, tok_s, tok_r, far_s, far_r, fwd_s, fwd_r,
    z_s, x_s, kv_r, o_s, o_r, ready,
    wg, ag, w_s, w_r, a_s, a_r,
):
    f32, bf16 = jnp.float32, jnp.bfloat16
    rows = tok.shape[0]
    half = 2 * rows
    block = 2 * half
    heads = wq.shape[1] // HD
    sp = lax.axis_index("sp")
    t = lax.axis_index("tp")
    core = lax.rem(t, 2)
    p = t // 2
    t1 = t + 1 - 2 * core
    t2 = lax.rem(t + 2, 4)
    t3 = 3 - t
    r = sp // 2
    c = lax.rem(sp, 2)
    last_row = sp_size // 2 - 1
    spx = sp + 1 - 2 * c
    has_next = r < last_row
    pa, pb = p, 1 - p

    def at(n, unit):
        return pl.ds(pl.multiple_of(n * unit, unit), unit)

    loads = [
        pltpu.make_async_copy(tok, x.at[at(t, rows)], load.at[0]),
        pltpu.make_async_copy(gate, gv, load.at[1]),
        pltpu.make_async_copy(wk, wboth.at[0:HD], load.at[2]),
        pltpu.make_async_copy(wv, wboth.at[HD : 2 * HD], load.at[3]),
        pltpu.make_async_copy(wq, wqv, load.at[4]),
        pltpu.make_async_copy(wo, wov, load.at[5]),
    ]
    for copy in loads:
        copy.start()

    barrier = pltpu.get_barrier_semaphore()
    pl.semaphore_signal(barrier, inc=1, device_id={"tp": t1}, device_id_type=MESH)
    pl.semaphore_signal(barrier, inc=1, device_id={"tp": t2}, device_id_type=MESH)
    pl.semaphore_signal(barrier, inc=1, device_id={"tp": t3}, device_id_type=MESH)
    pl.semaphore_signal(barrier, inc=1, device_id={"sp": spx}, device_id_type=MESH)

    @pl.when(has_next)
    def _():
        pl.semaphore_signal(barrier, inc=1, device_id={"sp": sp + 2}, device_id_type=MESH)

    @pl.when(r > 0)
    def _():
        pl.semaphore_signal(barrier, inc=1, device_id={"sp": sp - 2}, device_id_type=MESH)

    peers = 4 + jnp.where(has_next, 1, 0) + jnp.where(r > 0, 1, 0)
    pl.semaphore_wait(barrier, peers)

    step = rows // CHUNKS

    def piece(shard, n):
        return pl.ds(pl.multiple_of(shard * rows + n * step, step), step)

    def remote(src, dst, ss, rs, **where):
        return pltpu.make_async_remote_copy(
            src_ref=src, dst_ref=dst, send_sem=ss, recv_sem=rs,
            device_id=where, device_id_type=MESH,
        )

    far = []
    for n in range(CHUNKS):
        cp = remote(tok.at[pl.ds(n * step, step)], x.at[piece(t, n)], far_s.at[n], far_r.at[n], tp=t2)
        cp.start()
        far.append(cp)
    near = remote(tok, x.at[at(t, rows)], tok_s.at[0], tok_r.at[0], tp=t1)
    near.start()

    loads[1].wait()
    g = gv[...]
    hi = g.astype(bf16).astype(f32)
    mid = (g - hi).astype(bf16).astype(f32)
    low = (g - hi - mid).astype(bf16).astype(f32)
    parts = (hi, mid, low)
    extra = kv.shape[2] - 2 * HD
    index = lax.broadcasted_iota(jnp.int32, (extra, block), 0)
    key_side = jnp.where((index >= 3 * heads) & (index < 3 * heads + 3), 1.0, 0.0).astype(f32)
    for k in range(3):
        for h in range(heads):
            key_side = jnp.where(index == k * heads + h, -parts[k][h : h + 1, :], key_side)
    key_side = key_side.astype(bf16)
    kv[sp, 0, HD : HD + extra, :] = key_side[:, :half]
    kv[sp, 1, HD : HD + extra, :] = key_side[:, half:]
    for h in range(heads):
        side = jnp.where((index < 3 * heads) & (lax.rem(index, heads) == h), 1.0, 0.0).astype(f32)
        for k in range(3):
            side = jnp.where(index == 3 * heads + k, parts[k][h : h + 1, :], side)
        qt[h, HD : HD + extra, :] = side.astype(bf16)

    def project_kv(which):
        xs = x[at(which, half), :]
        both = lax.dot_general(
            wboth[...], xs, (((1,), (1,)), ((), ())), preferred_element_type=f32
        ).astype(bf16)
        kv[sp, which, 0:HD, :] = both[:HD]
        kv[sp, which, HD + extra :, :] = both[HD:]

    def project_q(which):
        xs = x[at(which, half), :]
        q = jnp.dot(xs, wqv[...], preferred_element_type=f32).astype(bf16).astype(f32)
        q = (q * (float(HD) ** -0.5)).T.astype(bf16)
        for h in range(heads):
            qt[h, 0:HD, at(which, half)] = q[h * HD : (h + 1) * HD]

    def along(src, which, row):
        ref = kv.at[src, which]
        return remote(ref, ref, z_s.at[row, which], kv_r.at[src, which], sp=2 * row + c)

    def across(src, which):
        ref = kv.at[src, which]
        return remote(ref, ref, x_s.at[src // 2, which], kv_r.at[src, which], sp=spx)

    def send_own(which):
        @pl.loop(0, last_row - r)
        def _(i):
            along(sp, which, last_row - i).start()

        @pl.when(c == 0)
        def _():
            across(sp, which).start()

    def relay(which):
        @pl.loop(1, r + 1)
        def _(i):
            across(sp - 2 * i, which).wait_recv()
            across(sp - 2 * i, which).start()

    def hear():
        @pl.when(r < last_row - 1)
        def _():
            pl.semaphore_wait(ready, 1)

    @pl.when(r > 0)
    def _():
        hear()

        @pl.when(has_next)
        def _():
            pl.semaphore_signal(ready, inc=1, device_id={"sp": sp - 2}, device_id_type=MESH)

    loads[0].wait()
    loads[2].wait()
    loads[3].wait()
    near.wait_recv()
    project_kv(pa)

    @pl.when(r == 0)
    def _():
        hear()

    send_own(pa)
    loads[4].wait()
    project_q(pa)

    fwd = []
    for n in range(CHUNKS):
        far[n].wait_recv()
        ref = x.at[piece(t2, n)]
        cp = remote(ref, ref, fwd_s.at[n], fwd_r.at[n], tp=t1)
        cp.start()
        fwd.append(cp)

    loads[5].wait()
    split = wo.shape[1] // 2
    gathered = pl.ds(0, split)
    w_far = remote(wov.at[:, gathered], wg.at[t], w_s.at[1], w_r.at[1], tp=t2)
    w_near = remote(wov.at[:, gathered], wg.at[t], w_s.at[0], w_r.at[0], tp=t1)
    w_far.start()

    for n in range(CHUNKS):
        fwd[n].wait_recv()
    w_near.start()
    project_kv(pb)
    send_own(pb)
    relay(pa)
    project_q(pb)

    def attend(src, diagonal):
        kt = jnp.concatenate([kv[src, 0, 0 : HD + extra, :], kv[src, 1, 0 : HD + extra, :]], axis=1)
        vt = jnp.concatenate([kv[src, 0, HD + extra :, :], kv[src, 1, HD + extra :, :]], axis=1)
        for h in range(heads):
            s = lax.dot_general(kt, qt[h], (((0,), (0,)), ((), ())), preferred_element_type=f32)
            lanes = slice(h * HD, (h + 1) * HD)
            if diagonal:
                key_pos = lax.broadcasted_iota(jnp.int32, s.shape, 0)
                query_pos = lax.broadcasted_iota(jnp.int32, s.shape, 1)
                s = jnp.where(key_pos <= query_pos, s, -jnp.inf)
                peak = jnp.max(s, axis=0, keepdims=True)
                w = jnp.exp(s - peak)
                tot[h : h + 1, :] = jnp.sum(w, axis=0, keepdims=True)
                acc[lanes, :] = jnp.dot(vt, w.astype(bf16), preferred_element_type=f32)
            else:
                before = top[h : h + 1, :]
                peak = jnp.maximum(before, jnp.max(s, axis=0, keepdims=True))
                w = jnp.exp(s - peak)
                decay = jnp.exp(before - peak)
                tot[h : h + 1, :] = tot[h : h + 1, :] * decay + jnp.sum(w, axis=0, keepdims=True)
                acc[lanes, :] = acc[lanes, :] * decay + jnp.dot(
                    vt, w.astype(bf16), preferred_element_type=f32
                )
            top[h : h + 1, :] = peak

    attend(sp, True)

    def wait_across(src):
        for which in (pa, pb):
            across(src, which).wait_recv()

    @pl.when(c == 1)
    def _():
        wait_across(spx)
        attend(spx, False)

    relay(pb)

    @pl.loop(1, r + 1)
    def _(i):
        attend(sp - 2 * i, False)

    @pl.loop(1, r + 1)
    def _(i):
        wait_across(spx - 2 * i)
        attend(spx - 2 * i, False)

    for h in range(heads):
        lanes = slice(h * HD, (h + 1) * HD)
        acc[lanes, :] = acc[lanes, :] / tot[h : h + 1, :]
    att[...] = acc[...].T.astype(bf16)
    exchange = []
    for n, peer in ((1, t2), (2, t3), (0, t1)):
        cp = remote(att.at[at(peer, rows)], ag.at[t], a_s.at[n], a_r.at[n], tp=peer)
        cp.start()
        exchange.append(cp)
    width = (wo.shape[1] - split) // CHUNKS
    near_sum, far_sum, own_sum = [], [], []
    for n in range(CHUNKS):
        cols = slice(split + n * width, split + (n + 1) * width)
        pf[:, cols] = jnp.dot(att[at(pb, half), :], wov[:, cols], preferred_element_type=f32)
        s_near[n] = pf[at(1 - core, rows), cols].astype(bf16)
        cp = remote(s_near.at[n], r_near.at[n], o_s.at[0, n], o_r.at[0, n], tp=t1)
        cp.start()
        near_sum.append(cp)
    for n in range(CHUNKS):
        cols = slice(split + n * width, split + (n + 1) * width)
        near_sum[n].wait_recv()
        s_far[n] = (pf[at(core, rows), cols] + r_near[n].astype(f32)).astype(bf16)
        cp = remote(s_far.at[n], r_far.at[n], o_s.at[1, n], o_r.at[1, n], tp=t2)
        cp.start()
        far_sum.append(cp)
    for n in range(CHUNKS):
        cols = slice(split + n * width, split + (n + 1) * width)
        own[:, cols] = jnp.dot(att[at(pa, half), :], wov[:, cols], preferred_element_type=f32)
        s_own[n] = own[at(1 - core, rows), cols].astype(bf16)
        cp = remote(s_own.at[n], r_own.at[n], o_s.at[2, n], o_r.at[2, n], tp=t1)
        cp.start()
        own_sum.append(cp)

    w_far.wait_recv()
    w_fwd = remote(wg.at[t2], wg.at[t2], w_s.at[2], w_r.at[2], tp=t1)
    w_fwd.start()
    total = jnp.dot(att[at(t, rows), :], wov[:, gathered], preferred_element_type=f32)
    for waits, peer in (((w_near, exchange[2]), t1), ((exchange[0],), t2), ((w_fwd, exchange[1]), t3)):
        for cp in waits:
            cp.wait_recv()
        total = total + jnp.dot(ag[peer], wg[peer], preferred_element_type=f32)
    out[:, gathered] = total.astype(bf16)
    for n in range(CHUNKS):
        cols = slice(split + n * width, split + (n + 1) * width)
        own_sum[n].wait_recv()
        far_sum[n].wait_recv()
        total = own[at(core, rows), cols] + r_own[n].astype(f32) + r_far[n].astype(f32)
        out[:, cols] = total.astype(bf16)

    near.wait_send()
    for cp in far + fwd + near_sum + far_sum + own_sum + exchange + [w_far, w_near, w_fwd]:
        cp.wait_send()
    for which in (pa, pb):

        @pl.when(c == 0)
        def _(which=which):
            across(sp, which).wait_send()

        @pl.loop(0, last_row - r)
        def _(i, which=which):
            along(sp, which, last_row - i).wait_send()

        @pl.loop(1, r + 1)
        def _(i, which=which):
            across(sp - 2 * i, which).wait_send()


def per_device(sp_size, tokens, w_query, w_key, w_value, w_out, cum_gate):
    rows, width = tokens.shape
    half, block = 2 * rows, 4 * rows
    heads = w_query.shape[1] // HD
    out_width = w_out.shape[1]
    extra = -(-(3 * heads + 3) // 16) * 16
    bf16, f32 = jnp.bfloat16, jnp.float32
    dma = pltpu.SemaphoreType.DMA
    anywhere = pl.BlockSpec(memory_space=pl.ANY)
    part = pltpu.VMEM((CHUNKS, rows, out_width // 2 // CHUNKS), bf16)
    return pl.pallas_call(
        functools.partial(kernel, sp_size),
        out_shape=jax.ShapeDtypeStruct((rows, out_width), bf16),
        in_specs=[anywhere] * 6,
        out_specs=pl.BlockSpec(memory_space=pltpu.VMEM),
        scratch_shapes=[
            pltpu.VMEM((block, width), bf16),
            pltpu.VMEM(w_query.shape, bf16),
            pltpu.VMEM((2 * HD, width), bf16),
            pltpu.VMEM(w_out.shape, bf16),
            pltpu.VMEM(cum_gate.shape, f32),
            pltpu.VMEM((sp_size, 2, 2 * HD + extra, half), bf16),
            pltpu.VMEM((heads, HD + extra, block), bf16),
            pltpu.VMEM((heads, block), f32),
            pltpu.VMEM((heads, block), f32),
            pltpu.VMEM((heads * HD, block), f32),
            pltpu.VMEM((block, heads * HD), bf16),
            pltpu.VMEM((half, out_width), f32),
            pltpu.VMEM((half, out_width), f32),
            part, part, part, part, part, part,
            dma((6,)),
            dma((1,)), dma((1,)),
            dma((CHUNKS,)), dma((CHUNKS,)),
            dma((CHUNKS,)), dma((CHUNKS,)),
            dma((sp_size // 2, 2)), dma((sp_size // 2, 2)), dma((sp_size, 2)),
            dma((3, CHUNKS)), dma((3, CHUNKS)),
            pltpu.SemaphoreType.REGULAR,
            pltpu.VMEM((4, w_out.shape[0], out_width // 2), bf16),
            pltpu.VMEM((4, rows, w_out.shape[0]), bf16),
            dma((3,)), dma((3,)), dma((3,)), dma((3,)),
        ],
        compiler_params=pltpu.CompilerParams(
            collective_id=0, has_side_effects=True, vmem_limit_bytes=62 * 1024 * 1024
        ),
    )(tokens, w_query, w_key.T, w_value.T, w_out, cum_gate)


def solution(mesh):
    placed = (
        P(("sp", "tp"), None),
        P(None, "tp"),
        P(None, "tp"),
        P(None, "tp"),
        P("tp", None),
        P("tp", "sp"),
    )
    return jax.shard_map(
        functools.partial(per_device, mesh.shape["sp"]),
        mesh=mesh, in_specs=placed, out_specs=P(("sp", "tp"), None), check_vma=False,
    )
```

profile of v0, /device:TPU:25, one launch (start us, length us, event | category | flops | bytes accessed | tf_op | source)
XLA Modules:
  0.0 31.0 jit_solution(16922195504489282933)
XLA Ops:
  0.0 29.4 %shard_map.64 = bf16[64,2048]{1,0:T(8,128)(2,1)} custom-call(bf16[64,2048]{1,0:T(8,128)(2,1)} %tok.1, bf16[2048,256]{1,0:T(8,128)(2,1)} %wq.1, bf16[64,2048]{1,0:T(8,128)(2,1)} %bitcast.2, bf16[64,2048]{1,0:T(8,128)(2,1)} %bitcast.3, bf16[256,2048]{1,0:T(8,128)(2,1)} %wo.1, f32[4,256]{1,0:T(4,128)} %gate.1), custom_call_target="tpu_custom_call" | custom-call | tf_op jit(solution)/shard_map/pallas_call | solution.py:325
  29.4 1.7 %copy.8 = bf16[64,2048]{1,0:T(8,128)(2,1)} copy(bf16[64,2048]{1,0:T(8,128)(2,1)} %shard_map.64) | data formatting | bytes 524288
where the time goes:
time: 31.6 us; the launch traced here: 31 us
  Pallas kernels  29.4 us (93%)
  local copies, waits for them, and re-layouts  1.67 us (5%)
    pallas_call x1, Pallas kernels, per_device(): pl.pallas_call(functools.partial(kernel, sp_size), out_shape=jax.ShapeDty...  29.4 us
    unnamed x1, local copies, waits for them, and re-layouts  1.67 us

commit v1 on v0

--- a/solution.py
+++ b/solution.py
@@ -320,11 +320,11 @@
     extra = -(-(3 * heads + 3) // 16) * 16
     bf16, f32 = jnp.bfloat16, jnp.float32
     dma = pltpu.SemaphoreType.DMA
-    anywhere = pl.BlockSpec(memory_space=pl.ANY)
+    anywhere = pl.BlockSpec(memory_space=pltpu.HBM)
     part = pltpu.VMEM((CHUNKS, rows, out_width // 2 // CHUNKS), bf16)
     return pl.pallas_call(
         functools.partial(kernel, sp_size),
-        out_shape=jax.ShapeDtypeStruct((rows, out_width), bf16),
+        out_shape=pltpu.VMEM((rows, out_width), bf16),
         in_specs=[anywhere] * 6,
         out_specs=pl.BlockSpec(memory_space=pltpu.VMEM),
         scratch_shapes=[

time: 31.6 us -> 29.9 us (0.946)
  local copies, waits for them, and re-layouts: 1.67 us -> 0.71 us
  Pallas kernels: 29.4 us -> 28.7 us
    unnamed x1, local copies, waits for them, and re-layouts: 1.67 us -> 0.71 us
    pallas_call x1, Pallas kernels: 29.4 us -> 28.7 us  [per_device(): pl.pallas_call(functools.partial(kernel, sp_size), out_shape=pltpu.VMEM((...]
where the time goes in v1:
time: 29.9 us; the launch traced here: 29.4 us
  Pallas kernels  28.7 us (96%)
  local copies, waits for them, and re-layouts  0.71 us (2%)
    pallas_call x1, Pallas kernels, per_device(): pl.pallas_call(functools.partial(kernel, sp_size), out_shape=pltpu.VMEM((...  28.7 us
    unnamed x1, local copies, waits for them, and re-layouts  0.71 us

profile of v1, /device:TPU:25, one launch (start us, length us, event | category | flops | bytes accessed | tf_op | source)
XLA Modules:
  0.0 29.4 jit_solution(7543018323474811561)
XLA Ops:
  0.0 28.7 %shard_map.64 = bf16[64,2048]{1,0:T(8,128)(2,1)S(1)} custom-call(bf16[64,2048]{1,0:T(8,128)(2,1)} %tok.1, bf16[2048,256]{1,0:T(8,128)(2,1)} %wq.1, bf16[64,2048]{1,0:T(8,128)(2,1)} %bitcast.2, bf16[64,2048]{1,0:T(8,128)(2,1)} %bitcast.3, bf16[256,2048]{1,0:T(8,128)(2,1)} %wo.1, f32[4,256]{1,0:T(4,128)} %gate.1), custom_call_target="tpu_custom_call" | custom-call | tf_op jit(solution)/shard_map/pallas_call | solution.py:325
  28.7 0.7 %copy.8 = bf16[64,2048]{1,0:T(8,128)(2,1)} copy(bf16[64,2048]{1,0:T(8,128)(2,1)S(1)} %shard_map.64) | data formatting | bytes 524288

commit v2 on v1

v2 whole, which is shorter than its diff:
```python
import functools

import jax
import jax.numpy as jnp
from jax import lax
from jax.experimental import pallas as pl
from jax.experimental.pallas import tpu as pltpu
from jax.sharding import PartitionSpec as P

HD = 64
MESH = pl.DeviceIdType.MESH
CHUNKS = 4
PARTS = 2
FAR = -1e30


def kernel(
    sp_size, tok, wq, wk, wv, wo, gate, out,
    x, wqv, wboth, gv, kv, qt, top, acc, att, part,
    s_far, r_far, wg, ag, ae,
    load, tok_s, tok_r, far_s, far_r, fwd_s, fwd_r,
    z_s, x_s, kv_r, o_s, o_r, ready, w_s, w_r, a_s, a_r,
):
    f32, bf16 = jnp.float32, jnp.bfloat16
    rows = tok.shape[0]
    half = 2 * rows
    block = 2 * half
    heads = wq.shape[1] // HD
    width = wo.shape[1]
    apart = s_far.shape[0] * s_far.shape[2]
    gathered = pl.ds(0, width - apart)
    sp = lax.axis_index("sp")
    t = lax.axis_index("tp")
    core = lax.rem(t, 2)
    p = t // 2
    t1 = t + 1 - 2 * core
    t2 = lax.rem(t + 2, 4)
    t3 = 3 - t
    r = sp // 2
    c = lax.rem(sp, 2)
    last_row = sp_size // 2 - 1
    spx = sp + 1 - 2 * c
    has_next = r < last_row
    pa, pb = p, 1 - p

    def at(n, unit):
        return pl.ds(pl.multiple_of(n * unit, unit), unit)

    loads = [
        pltpu.make_async_copy(tok, x.at[at(t, rows)], load.at[0]),
        pltpu.make_async_copy(gate, gv, load.at[1]),
        pltpu.make_async_copy(wk, wboth.at[0:HD], load.at[2]),
        pltpu.make_async_copy(wv, wboth.at[HD : 2 * HD], load.at[3]),
        pltpu.make_async_copy(wq, wqv, load.at[4]),
        pltpu.make_async_copy(wo, wg.at[t], load.at[5]),
    ]
    for copy in loads:
        copy.start()

    barrier = pltpu.get_barrier_semaphore()
    pl.semaphore_signal(barrier, inc=1, device_id={"tp": t1}, device_id_type=MESH)
    pl.semaphore_signal(barrier, inc=1, device_id={"tp": t2}, device_id_type=MESH)
    pl.semaphore_signal(barrier, inc=1, device_id={"tp": t3}, device_id_type=MESH)
    pl.semaphore_signal(barrier, inc=1, device_id={"sp": spx}, device_id_type=MESH)

    @pl.when(has_next)
    def _():
        pl.semaphore_signal(barrier, inc=1, device_id={"sp": sp + 2}, device_id_type=MESH)

    @pl.when(r > 0)
    def _():
        pl.semaphore_signal(barrier, inc=1, device_id={"sp": sp - 2}, device_id_type=MESH)

    loads[0].wait()
    peers = 4 + jnp.where(has_next, 1, 0) + jnp.where(r > 0, 1, 0)
    pl.semaphore_wait(barrier, peers)

    step = rows // CHUNKS

    def piece(shard, n):
        return pl.ds(pl.multiple_of(shard * rows + n * step, step), step)

    def remote(src, dst, ss, rs, **where):
        return pltpu.make_async_remote_copy(
            src_ref=src, dst_ref=dst, send_sem=ss, recv_sem=rs,
            device_id=where, device_id_type=MESH,
        )

    far = []
    for n in range(CHUNKS):
        ref = x.at[piece(t, n)]
        cp = remote(ref, ref, far_s.at[n], far_r.at[n], tp=t2)
        cp.start()
        far.append(cp)
    mine = x.at[at(t, rows)]
    near = remote(mine, mine, tok_s.at[0], tok_r.at[0], tp=t1)
    near.start()

    loads[1].wait()
    g = gv[...]
    hi = g.astype(bf16).astype(f32)
    mid = (g - hi).astype(bf16).astype(f32)
    low = (g - hi - mid).astype(bf16).astype(f32)
    parts = (hi, mid, low)
    extra = kv.shape[2] - 2 * HD
    index = lax.broadcasted_iota(jnp.int32, (extra, block), 0)
    key_side = jnp.where((index >= 3 * heads) & (index < 3 * heads + 3), 1.0, 0.0).astype(f32)
    for k in range(3):
        for h in range(heads):
            key_side = jnp.where(index == k * heads + h, -parts[k][h : h + 1, :], key_side)
    key_side = key_side.astype(bf16)
    kv[sp, 0, HD : HD + extra, :] = key_side[:, :half]
    kv[sp, 1, HD : HD + extra, :] = key_side[:, half:]
    for h in range(heads):
        side = jnp.where((index < 3 * heads) & (lax.rem(index, heads) == h), 1.0, 0.0).astype(f32)
        for k in range(3):
            side = jnp.where(index == 3 * heads + k, parts[k][h : h + 1, :], side)
        side = side.astype(bf16)
        for which in range(2):
            qt[which, HD : HD + extra, h * half : (h + 1) * half] = side[:, which * half : (which + 1) * half]

    def project_kv(which):
        xs = x[at(which, half), :]
        both = lax.dot_general(
            wboth[...], xs, (((1,), (1,)), ((), ())), preferred_element_type=f32
        ).astype(bf16)
        kv[sp, which, 0:HD, :] = both[:HD]
        kv[sp, which, HD + extra :, :] = both[HD:]

    def project_q(which):
        xs = x[at(which, half), :]
        q = jnp.dot(xs, wqv[...], preferred_element_type=f32).astype(bf16).astype(f32)
        q = (q * (float(HD) ** -0.5)).T.astype(bf16)
        for h in range(heads):
            qt[which, 0:HD, h * half : (h + 1) * half] = q[h * HD : (h + 1) * HD]

    def along(src, which, row):
        ref = kv.at[src, which]
        return remote(ref, ref, z_s.at[row, which], kv_r.at[src, which], sp=2 * row + c)

    def across(src, which):
        ref = kv.at[src, which]
        return remote(ref, ref, x_s.at[src // 2, which], kv_r.at[src, which], sp=spx)

    def send_own(which):
        @pl.loop(0, last_row - r)
        def _(i):
            along(sp, which, last_row - i).start()

        @pl.when(c == 0)
        def _():
            across(sp, which).start()

    def hear():
        @pl.when(r < last_row - 1)
        def _():
            pl.semaphore_wait(ready, 1)

    @pl.when(r > 0)
    def _():
        hear()

        @pl.when(has_next)
        def _():
            pl.semaphore_signal(ready, inc=1, device_id={"sp": sp - 2}, device_id_type=MESH)

    def absorb(*groups, first=False, masked=False):
        scores = []
        for which, pieces in groups:
            q = qt[which]
            for src, kind in pieces:
                s = lax.dot_general(
                    kv[src, kind, 0 : HD + extra, :], q, (((0,), (0,)), ((), ())),
                    preferred_element_type=f32,
                )
                if src is sp and masked:
                    key_pos = lax.broadcasted_iota(jnp.int32, s.shape, 0) + kind * half
                    query_pos = lax.broadcasted_iota(jnp.int32, s.shape, 1) % half + which * half
                    s = jnp.where(key_pos <= query_pos, s, FAR)
                scores.append(s)
        tops, n = [], 0
        for which, pieces in groups:
            peak = None if first else top[which, 0:1, :]
            for _ in pieces:
                high = jnp.max(scores[n], axis=0, keepdims=True)
                peak = high if peak is None else jnp.maximum(peak, high)
                n += 1
            tops.append(peak)
        weights, n = [], 0
        for peak, (which, pieces) in zip(tops, groups):
            for _ in pieces:
                weights.append(jnp.exp(scores[n] - peak).astype(bf16))
                n += 1
        n = 0
        for peak, (which, pieces) in zip(tops, groups):
            total = None
            for src, kind in pieces:
                term = jnp.dot(kv[src, kind, HD:, :], weights[n], preferred_element_type=f32)
                total = term if total is None else total + term
                n += 1
            if not first:
                total = total + acc[which] * jnp.exp(top[which, 0:1, :] - peak)
            acc[which] = total
            top[which, 0:1, :] = peak

    def over(work):
        @pl.loop(0, r // 3)
        def _(j):
            work([3 * j + 1, 3 * j + 2, 3 * j + 3])

        @pl.when(r % 3 == 1)
        def _():
            work([r])

        @pl.when(r % 3 == 2)
        def _():
            work([r - 1, r])

    def forward(n):
        far[n].wait_recv()
        ref = x.at[piece(t2, n)]
        cp = remote(ref, ref, fwd_s.at[n], fwd_r.at[n], tp=t1)
        cp.start()
        return cp

    loads[2].wait()
    loads[3].wait()
    near.wait_recv()
    project_kv(pa)

    @pl.when(r == 0)
    def _():
        hear()

    send_own(pa)
    loads[4].wait()
    project_q(pa)
    loads[5].wait()
    w_near = remote(wg.at[t], wg.at[t], w_s.at[0], w_r.at[0], tp=t1)
    w_near.start()
    absorb((pa, [(sp, pa)]), first=True, masked=True)
    fwd = [forward(0), forward(1)]

    @pl.when(c == 1)
    def _():
        across(spx, pa).wait_recv()
        absorb((pa, [(spx, pa)]))

    def relay(which):
        @pl.loop(1, r + 1)
        def _(i):
            across(sp - 2 * i, which).wait_recv()
            across(sp - 2 * i, which).start()

    relay(pa)
    fwd.append(forward(2))
    w_far = remote(wg.at[t, :, gathered], wg.at[t, :, gathered], w_s.at[1], w_r.at[1], tp=t2)
    w_far.start()
    over(lambda ids: absorb((pa, [(sp - 2 * i, pa) for i in ids])))
    fwd.append(forward(3))
    for cp in fwd:
        cp.wait_recv()
    project_kv(pb)
    send_own(pb)
    project_q(pb)

    @pl.when(c == 0)
    def _():
        absorb((pb, [(sp, pa)]), first=True, masked=True)

    @pl.when(c == 1)
    def _():
        absorb((pb, [(sp, pa), (spx, pa)]), first=True, masked=True)

    def earlier(ids):
        for i in ids:
            across(spx - 2 * i, pa).wait_recv()
        direct = [(sp - 2 * i, pa) for i in ids]
        relayed = [(spx - 2 * i, pa) for i in ids]
        absorb((pb, direct + relayed), (pa, relayed))

    over(earlier)

    @pl.when(c == 0)
    def _():
        absorb((pb, [(sp, pb)]), (pa, [(sp, pb)]), masked=True)

    @pl.when(c == 1)
    def _():
        across(spx, pb).wait_recv()
        both = [(sp, pb), (spx, pb)]
        absorb((pb, both), (pa, both), masked=True)

    relay(pb)

    def directs(ids):
        pieces = [(sp - 2 * i, pb) for i in ids]
        absorb((pb, pieces), (pa, pieces))

    over(directs)

    def lasts(ids):
        for i in ids:
            across(spx - 2 * i, pb).wait_recv()
        absorb((pb, [(spx - 2 * i, pb) for i in ids]))

    over(lasts)

    def settle(which):
        total = acc[which, 3 * heads : 3 * heads + 1, :]
        rest = acc[which, extra : extra + HD, :] / total
        heads_up = jnp.concatenate([rest[:, h * half : (h + 1) * half] for h in range(heads)], axis=0)
        att[which] = heads_up.T.astype(bf16)

    settle(pb)
    theirs, others = att.at[pb, at(core, rows)], att.at[pb, at(1 - core, rows)]
    ex_pair = remote(others, ae, a_s.at[3], a_r.at[3], tp=t1)
    ex_pair.start()
    ex_far = remote(theirs, ag.at[t], a_s.at[1], a_r.at[1], tp=t2)
    ex_far.start()
    ex_skew = remote(others, ag.at[t], a_s.at[2], a_r.at[2], tp=t3)
    ex_skew.start()

    over(lambda ids: absorb((pa, [(spx - 2 * i, pb) for i in ids])))
    w_near.wait_recv()
    ex_pair.wait_recv()
    sums = []
    each = s_far.shape[2]
    for n in range(PARTS):
        cols = slice(width - apart + n * each, width - apart + (n + 1) * each)
        both = jnp.dot(att[pb, at(core, rows), :], wg[t, :, cols], preferred_element_type=f32)
        both += jnp.dot(ae[...], wg[t1, :, cols], preferred_element_type=f32)
        s_far[n] = both.astype(bf16)
        cp = remote(s_far.at[n], r_far.at[n], o_s.at[n], o_r.at[n], tp=t2)
        cp.start()
        sums.append(cp)

    settle(pa)
    ex_near = remote(att.at[pa, at(1 - core, rows)], ag.at[t], a_s.at[0], a_r.at[0], tp=t1)
    ex_near.start()
    w_far.wait_recv()
    w_fwd = remote(wg.at[t2, :, gathered], wg.at[t2, :, gathered], w_s.at[2], w_r.at[2], tp=t1)
    w_fwd.start()
    part[...] = jnp.dot(att[pa, at(core, rows), :], wg[t], preferred_element_type=f32)
    ex_near.wait_recv()
    part[...] += jnp.dot(ag[t1], wg[t1], preferred_element_type=f32)
    ex_far.wait_recv()
    total = part[:, gathered] + jnp.dot(ag[t2], wg[t2, :, gathered], preferred_element_type=f32)
    ex_skew.wait_recv()
    w_fwd.wait_recv()
    total = total + jnp.dot(ag[t3], wg[t3, :, gathered], preferred_element_type=f32)
    out[:, gathered] = total.astype(bf16)
    for n in range(PARTS):
        cols = slice(width - apart + n * each, width - apart + (n + 1) * each)
        sums[n].wait_recv()
        out[:, cols] = (part[:, cols] + r_far[n].astype(f32)).astype(bf16)

    for cp in [near, w_near, w_far, w_fwd, ex_pair, ex_far, ex_skew, ex_near] + far + fwd + sums:
        cp.wait_send()
    for which in (pa, pb):

        @pl.when(c == 0)
        def _(which=which):
            across(sp, which).wait_send()

        @pl.loop(0, last_row - r)
        def _(i, which=which):
            along(sp, which, last_row - i).wait_send()

        @pl.loop(1, r + 1)
        def _(i, which=which):
            across(sp - 2 * i, which).wait_send()


def per_device(sp_size, tokens, w_query, w_key, w_value, w_out, cum_gate):
    rows, width = tokens.shape
    half, block = 2 * rows, 4 * rows
    heads = w_query.shape[1] // HD
    out_width = w_out.shape[1]
    extra = -(-(3 * heads + 3) // 16) * 16
    bf16, f32 = jnp.bfloat16, jnp.float32
    dma = pltpu.SemaphoreType.DMA
    anywhere = pl.BlockSpec(memory_space=pltpu.HBM)
    strip = pltpu.VMEM((PARTS, rows, out_width * 5 // 16), bf16)
    return pl.pallas_call(
        functools.partial(kernel, sp_size),
        out_shape=pltpu.VMEM((rows, out_width), bf16),
        in_specs=[anywhere] * 6,
        out_specs=pl.BlockSpec(memory_space=pltpu.VMEM),
        scratch_shapes=[
            pltpu.VMEM((block, width), bf16),
            pltpu.VMEM(w_query.shape, bf16),
            pltpu.VMEM((2 * HD, width), bf16),
            pltpu.VMEM(cum_gate.shape, f32),
            pltpu.VMEM((sp_size, 2, 2 * HD + extra, half), bf16),
            pltpu.VMEM((2, HD + extra, heads * half), bf16),
            pltpu.VMEM((2, 8, heads * half), f32),
            pltpu.VMEM((2, HD + extra, heads * half), f32),
            pltpu.VMEM((2, half, heads * HD), bf16),
            pltpu.VMEM((rows, out_width), f32),
            strip, strip,
            pltpu.VMEM((4,) + w_out.shape, bf16),
            pltpu.VMEM((4, rows, w_out.shape[0]), bf16),
            pltpu.VMEM((rows, w_out.shape[0]), bf16),
            dma((6,)),
            dma((1,)), dma((1,)),
            dma((CHUNKS,)), dma((CHUNKS,)),
            dma((CHUNKS,)), dma((CHUNKS,)),
            dma((sp_size // 2, 2)), dma((sp_size // 2, 2)), dma((sp_size, 2)),
            dma((PARTS,)), dma((PARTS,)),
            pltpu.SemaphoreType.REGULAR,
            dma((3,)), dma((3,)), dma((4,)), dma((4,)),
        ],
        compiler_params=pltpu.CompilerParams(
            collective_id=0, has_side_effects=True, vmem_limit_bytes=62 * 1024 * 1024
        ),
    )(tokens, w_query, w_key.T, w_value.T, w_out, cum_gate)


def solution(mesh):
    placed = (
        P(("sp", "tp"), None),
        P(None, "tp"),
        P(None, "tp"),
        P(None, "tp"),
        P("tp", None),
        P("tp", "sp"),
    )
    return jax.shard_map(
        functools.partial(per_device, mesh.shape["sp"]),
        mesh=mesh, in_specs=placed, out_specs=P(("sp", "tp"), None), check_vma=False,
    )
```

time: 29.9 us -> 28.5 us (0.953)
  Pallas kernels: 28.7 us -> 27.3 us
    pallas_call x1, Pallas kernels: 28.7 us -> 27.3 us  [per_device(): pl.pallas_call(functools.partial(kernel, sp_size), out_shape=pltpu.VMEM((...]
where the time goes in v2:
time: 28.5 us; the launch traced here: 28 us
  Pallas kernels  27.3 us (96%)
  local copies, waits for them, and re-layouts  0.71 us (2%)
    pallas_call x1, Pallas kernels, per_device(): pl.pallas_call(functools.partial(kernel, sp_size), out_shape=pltpu.VMEM((...  27.3 us
    unnamed x1, local copies, waits for them, and re-layouts  0.71 us

profile of v2, /device:TPU:25, one launch (start us, length us, event | category | flops | bytes accessed | tf_op | source)
XLA Modules:
  0.0 28.0 jit_solution(17577899245792859065)
XLA Ops:
  0.0 27.3 %shard_map.64 = bf16[64,2048]{1,0:T(8,128)(2,1)S(1)} custom-call(bf16[64,2048]{1,0:T(8,128)(2,1)} %tok.1, bf16[2048,256]{1,0:T(8,128)(2,1)} %wq.1, bf16[64,2048]{1,0:T(8,128)(2,1)} %bitcast.2, bf16[64,2048]{1,0:T(8,128)(2,1)} %bitcast.3, bf16[256,2048]{1,0:T(8,128)(2,1)} %wo.1, f32[4,256]{1,0:T(4,128)} %gate.1), custom_call_target="tpu_custom_call" | custom-call | tf_op jit(solution)/shard_map/pallas_call | solution.py:385
  27.3 0.7 %copy.8 = bf16[64,2048]{1,0:T(8,128)(2,1)} copy(bf16[64,2048]{1,0:T(8,128)(2,1)S(1)} %shard_map.64) | data formatting | bytes 524288

commit v3 on v2

v3 whole, which is shorter than its diff:
```python
import functools

import jax
import jax.numpy as jnp
from jax import lax
from jax.experimental import pallas as pl
from jax.experimental.pallas import tpu as pltpu
from jax.sharding import PartitionSpec as P

HD = 64
MESH = pl.DeviceIdType.MESH
CHUNKS = 4
GROUPS = 2
PARTS = 2
FAR = -1e30


def kernel(
    sp_size, tok, wq, wk, wv, wo, gate, out,
    x, wqv, wboth, gv, kv, gk, qt, top, acc, att, part,
    s_far, r_far, wg, ag, ae,
    load, tok_s, tok_r, far_s, far_r, fwd_s, fwd_r,
    z_s, x_s, kv_r, o_s, o_r, ready, w_s, w_r, a_s, a_r,
):
    f32, bf16 = jnp.float32, jnp.bfloat16
    rows = tok.shape[0]
    half = 2 * rows
    block = 2 * half
    heads = wq.shape[1] // HD
    width = wo.shape[1]
    apart = s_far.shape[0] * s_far.shape[2]
    gathered = pl.ds(0, width - apart)
    sp = lax.axis_index("sp")
    t = lax.axis_index("tp")
    core = lax.rem(t, 2)
    p = t // 2
    t1 = t + 1 - 2 * core
    t2 = lax.rem(t + 2, 4)
    t3 = 3 - t
    r = sp // 2
    c = lax.rem(sp, 2)
    last_row = sp_size // 2 - 1
    spx = sp + 1 - 2 * c
    has_next = r < last_row

    def at(n, unit):
        return pl.ds(pl.multiple_of(n * unit, unit), unit)

    span = rows // GROUPS
    loads = [
        pltpu.make_async_copy(gate, gv, load.at[0]),
        pltpu.make_async_copy(wk, wboth.at[0:HD], load.at[1]),
        pltpu.make_async_copy(wv, wboth.at[HD : 2 * HD], load.at[2]),
        pltpu.make_async_copy(wq, wqv, load.at[3]),
        pltpu.make_async_copy(wo, wg.at[t], load.at[4]),
    ]
    arrive = [
        pltpu.make_async_copy(tok.at[pl.ds(n * span, span)], x.at[0, n, core], load.at[5 + n])
        for n in range(GROUPS)
    ]
    for copy in arrive:
        copy.start()
    for copy in loads:
        copy.start()

    barrier = pltpu.get_barrier_semaphore()
    pl.semaphore_signal(barrier, inc=1, device_id={"tp": t1}, device_id_type=MESH)
    pl.semaphore_signal(barrier, inc=1, device_id={"tp": t2}, device_id_type=MESH)
    pl.semaphore_signal(barrier, inc=1, device_id={"tp": t3}, device_id_type=MESH)
    pl.semaphore_signal(barrier, inc=1, device_id={"sp": spx}, device_id_type=MESH)

    @pl.when(has_next)
    def _():
        pl.semaphore_signal(barrier, inc=1, device_id={"sp": sp + 2}, device_id_type=MESH)

    @pl.when(r > 0)
    def _():
        pl.semaphore_signal(barrier, inc=1, device_id={"sp": sp - 2}, device_id_type=MESH)

    for copy in arrive:
        copy.wait()
    peers = 4 + jnp.where(has_next, 1, 0) + jnp.where(r > 0, 1, 0)
    pl.semaphore_wait(barrier, peers)

    step = rows // CHUNKS

    def piece(kind, n):
        return x.at[kind, n * step // span, core, pl.ds(n * step % span, step)]

    def remote(src, dst, ss, rs, **where):
        return pltpu.make_async_remote_copy(
            src_ref=src, dst_ref=dst, send_sem=ss, recv_sem=rs,
            device_id=where, device_id_type=MESH,
        )

    far = []
    for n in range(CHUNKS):
        cp = remote(piece(0, n), piece(1, n), far_s.at[n], far_r.at[n], tp=t2)
        cp.start()
        far.append(cp)
    mine = x.at[0, :, core]
    near = remote(mine, mine, tok_s.at[0], tok_r.at[0], tp=t1)
    near.start()

    def place(n):
        return lax.rem(n // span, 2) * rows + n // (2 * span) * span + lax.rem(n, span)

    loads[0].wait()
    g = gv[...]
    lanes = [slice(core_n * rows + n * span, core_n * rows + (n + 1) * span) for n in range(GROUPS) for core_n in range(2)]
    sides = (jnp.where(p == 0, g[:, :half], g[:, half:]), jnp.where(p == 0, g[:, half:], g[:, :half]))
    extra = (kv.shape[1] - block) // 2
    zeros = jnp.zeros(gk.shape[2:], bf16)
    index = lax.broadcasted_iota(jnp.int32, (extra, half), 0)
    for kind, gs in enumerate(sides):
        gs = jnp.concatenate([gs[:, cut] for cut in lanes], axis=1)
        hi = gs.astype(bf16).astype(f32)
        mid = (gs - hi).astype(bf16).astype(f32)
        low = (gs - hi - mid).astype(bf16).astype(f32)
        parts = (hi, mid, low)
        key_side = jnp.where((index >= 3 * heads) & (index < 3 * heads + 3), 1.0, 0.0).astype(f32)
        for k in range(3):
            for h in range(heads):
                key_side = jnp.where(index == k * heads + h, -parts[k][h : h + 1, :], key_side)
        kv[sp, kind * extra : (kind + 1) * extra, :] = key_side.astype(bf16)
        qt[kind] = jnp.zeros(qt.shape[1:], bf16)
        for h in range(heads):
            side = jnp.where((index < 3 * heads) & (lax.rem(index, heads) == h), 1.0, 0.0).astype(f32)
            for k in range(3):
                side = jnp.where(index == 3 * heads + k, parts[k][h : h + 1, :], side)
            qt[kind, 2 * HD : 2 * HD + extra, h * half : (h + 1) * half] = side.astype(bf16)

    def unpack(src):
        for kind in range(2):
            lines = kv[src, kind * extra : (kind + 1) * extra, :]
            wide = jnp.concatenate([lines, jnp.zeros((gk.shape[2] - extra, half), bf16)], axis=0)
            gk[src, kind * half : (kind + 1) * half, :] = wide.T

    bounds = (0, half, half + half // GROUPS, block)
    lead = 2 * extra

    def project_kv(part_n):
        lo, hi_row = bounds[part_n], bounds[part_n + 1]
        xs = x[0] if part_n == 0 else x[1, part_n - 1]
        both = lax.dot_general(
            xs.reshape(hi_row - lo, x.shape[-1]), wboth[...], (((1,), (1,)), ((), ())),
            preferred_element_type=f32,
        )
        kv[sp, lead + lo : lead + hi_row, :] = both.astype(bf16)

    def project_q(kind):
        xs = x[kind].reshape(half, x.shape[-1])
        q = jnp.dot(xs, wqv[...], preferred_element_type=f32).astype(bf16).astype(f32)
        q = (q * (float(HD) ** -0.5)).T.astype(bf16)
        for h in range(heads):
            qt[kind, 0:HD, h * half : (h + 1) * half] = q[h * HD : (h + 1) * HD]

    def message(src, n):
        return kv.at[src, 0 if n == 0 else lead + bounds[n] : lead + bounds[n + 1]]

    def along(src, n, row):
        ref = message(src, n)
        return remote(ref, ref, z_s.at[row, n], kv_r.at[src, n], sp=2 * row + c)

    def across(src, n):
        ref = message(src, n)
        return remote(ref, ref, x_s.at[src // 2, n], kv_r.at[src, n], sp=spx)

    def send_own(n):
        @pl.loop(0, last_row - r)
        def _(i):
            along(sp, n, last_row - i).start()

        @pl.when(c == 0)
        def _():
            across(sp, n).start()

    def hear():
        @pl.when(r < last_row - 1)
        def _():
            pl.semaphore_wait(ready, 1)

    @pl.when(r > 0)
    def _():
        hear()

        @pl.when(has_next)
        def _():
            pl.semaphore_signal(ready, inc=1, device_id={"sp": sp - 2}, device_id_type=MESH)

    def positions(shape, axis, kind, offset):
        n = lax.rem(lax.broadcasted_iota(jnp.int32, shape, axis), half) + offset
        return place(n) + (p if kind == 0 else 1 - p) * half

    def absorb(*groups, first=()):
        held = {}
        scores = []
        for kind, pieces in groups:
            name = tuple((id(src), lo, hi_row) for src, lo, hi_row in pieces)
            if name not in held:
                keys = jnp.concatenate([kv[src, lead + lo : lead + hi_row, :] for src, lo, hi_row in pieces], axis=0)
                tails = jnp.concatenate([gk[src, lo:hi_row, :] for src, lo, hi_row in pieces], axis=0)
                ones = jnp.ones((16, keys.shape[0]), bf16)
                held[name] = (
                    jnp.concatenate([keys, tails], axis=1),
                    jnp.concatenate([keys.T[HD:], ones], axis=0),
                )
            s = jnp.dot(held[name][0], qt[kind], preferred_element_type=f32)
            cuts, n = [], 0
            for src, lo, hi_row in pieces:
                cut = s[n : n + hi_row - lo]
                n += hi_row - lo
                if src is sp:
                    key_kind = 0 if lo < half else 1
                    key_pos = positions((cut.shape[0], 1), 0, key_kind, lo % half)
                    query_pos = positions((1, cut.shape[1]), 1, kind, 0)
                    cut = jnp.where(key_pos <= query_pos, cut, FAR)
                cuts.append(cut)
            scores.append((name, cuts))
        tops = []
        for (kind, _), (_, cuts) in zip(groups, scores):
            peak = None if kind in first else top[kind, 0:1, :]
            for s in cuts:
                high = jnp.max(s, axis=0, keepdims=True)
                peak = high if peak is None else jnp.maximum(peak, high)
            tops.append(peak)
        weights = [
            jnp.concatenate([jnp.exp(s - peak).astype(bf16) for s in cuts], axis=0)
            for peak, (_, cuts) in zip(tops, scores)
        ]
        for peak, w, (kind, _), (name, _) in zip(tops, weights, groups, scores):
            total = jnp.dot(held[name][1], w, preferred_element_type=f32)
            if kind not in first:
                total = total + acc[kind] * jnp.exp(top[kind, 0:1, :] - peak)
            acc[kind] = total
            top[kind, 0:1, :] = peak

    def over(work):
        @pl.loop(0, r // 3)
        def _(j):
            work([3 * j + 1, 3 * j + 2, 3 * j + 3])

        @pl.when(r % 3 == 1)
        def _():
            work([r])

        @pl.when(r % 3 == 2)
        def _():
            work([r - 1, r])

    def forward(n):
        far[n].wait_recv()
        cp = remote(piece(1, n), piece(1, n), fwd_s.at[n], fwd_r.at[n], tp=t1)
        cp.start()
        return cp

    def relay(n):
        @pl.loop(1, r + 1)
        def _(i):
            across(sp - 2 * i, n).wait_recv()
            across(sp - 2 * i, n).start()

    first_part, early, late, other = [(0, half), (half, bounds[2]), (bounds[2], block), (half, block)]

    loads[1].wait()
    loads[2].wait()
    near.wait_recv()
    project_kv(0)

    @pl.when(r == 0)
    def _():
        hear()

    send_own(0)
    loads[3].wait()
    project_q(0)
    loads[4].wait()
    w_near = remote(wg.at[t], wg.at[t], w_s.at[0], w_r.at[0], tp=t1)
    w_near.start()
    unpack(sp)
    absorb((0, [(sp, *first_part)]), first=(0,))
    fwd = [forward(0), forward(1)]

    @pl.when(c == 1)
    def _():
        across(spx, 0).wait_recv()
        unpack(spx)
        absorb((0, [(spx, *first_part)]))

    relay(0)
    fwd[0].wait_recv()
    fwd[1].wait_recv()
    project_kv(1)
    send_own(1)
    fwd.append(forward(2))
    w_far = remote(wg.at[t, :, gathered], wg.at[t, :, gathered], w_s.at[1], w_r.at[1], tp=t2)
    w_far.start()

    def directs(ids):
        srcs = [sp - 2 * i for i in ids]
        for src in srcs:
            unpack(src)
        absorb((0, [(src, *first_part) for src in srcs]))

    over(directs)
    fwd.append(forward(3))
    absorb((0, [(sp, *early)]))
    fwd[2].wait_recv()
    fwd[3].wait_recv()
    project_kv(2)
    send_own(2)
    project_q(1)
    relay(1)

    @pl.when(c == 0)
    def _():
        absorb((1, [(sp, *first_part), (sp, *other)]), (0, [(sp, *late)]), first=(1,))

    @pl.when(c == 1)
    def _():
        across(spx, 1).wait_recv()
        absorb(
            (1, [(sp, *first_part), (sp, *other), (spx, 0, bounds[2])]),
            (0, [(sp, *late), (spx, *early)]), first=(1,),
        )

    def mixed(ids):
        near_by, beyond = [sp - 2 * i for i in ids], [spx - 2 * i for i in ids]
        for src in beyond:
            across(src, 0).wait_recv()
            unpack(src)
        absorb(
            (1, [(src, 0, bounds[2]) for src in near_by] + [(src, *first_part) for src in beyond]),
            (0, [(src, *early) for src in near_by] + [(src, *first_part) for src in beyond]),
        )

    over(mixed)

    @pl.when(c == 1)
    def _():
        across(spx, 2).wait_recv()
        absorb((1, [(spx, *late)]), (0, [(spx, *late)]))

    relay(2)

    def nearly(ids):
        near_by, beyond = [sp - 2 * i for i in ids], [spx - 2 * i for i in ids]
        for src in beyond:
            across(src, 1).wait_recv()
        pieces = [(src, *late) for src in near_by] + [(src, *early) for src in beyond]
        absorb((1, pieces), (0, pieces))

    over(nearly)

    def lasts(ids):
        beyond = [spx - 2 * i for i in ids]
        for src in beyond:
            across(src, 2).wait_recv()
        absorb((1, [(src, *late) for src in beyond]))

    over(lasts)

    def settle(kind):
        rest = acc[kind, 0:HD, :] / acc[kind, HD : HD + 1, :]
        heads_up = jnp.concatenate([rest[:, h * half : (h + 1) * half] for h in range(heads)], axis=0)
        att[kind] = heads_up.T.astype(bf16).reshape(att.shape[1:])

    settle(1)
    theirs, others = att.at[1, :, core], att.at[1, :, 1 - core]
    ex_pair = remote(others, ae, a_s.at[3], a_r.at[3], tp=t1)
    ex_pair.start()
    ex_far = remote(theirs, ag.at[t], a_s.at[1], a_r.at[1], tp=t2)
    ex_far.start()
    ex_skew = remote(others, ag.at[t], a_s.at[2], a_r.at[2], tp=t3)
    ex_skew.start()
    over(lambda ids: absorb((0, [(spx - 2 * i, *late) for i in ids])))

    def flat(value):
        return value.reshape(rows, value.shape[-1])

    w_near.wait_recv()
    ex_pair.wait_recv()
    sums = []
    each = s_far.shape[2]
    for n in range(PARTS):
        cols = slice(width - apart + n * each, width - apart + (n + 1) * each)
        both = jnp.dot(flat(att[1, :, core]), wg[t, :, cols], preferred_element_type=f32)
        both += jnp.dot(flat(ae[...]), wg[t1, :, cols], preferred_element_type=f32)
        s_far[n] = both.astype(bf16)
        cp = remote(s_far.at[n], r_far.at[n], o_s.at[n], o_r.at[n], tp=t2)
        cp.start()
        sums.append(cp)

    settle(0)
    ex_near = remote(att.at[0, :, 1 - core], ag.at[t], a_s.at[0], a_r.at[0], tp=t1)
    ex_near.start()
    w_far.wait_recv()
    w_fwd = remote(wg.at[t2, :, gathered], wg.at[t2, :, gathered], w_s.at[2], w_r.at[2], tp=t1)
    w_fwd.start()
    part[...] = jnp.dot(flat(att[0, :, core]), wg[t], preferred_element_type=f32)
    ex_near.wait_recv()
    part[...] += jnp.dot(flat(ag[t1]), wg[t1], preferred_element_type=f32)
    ex_far.wait_recv()
    total = part[:, gathered] + jnp.dot(flat(ag[t2]), wg[t2, :, gathered], preferred_element_type=f32)
    ex_skew.wait_recv()
    w_fwd.wait_recv()
    total = total + jnp.dot(flat(ag[t3]), wg[t3, :, gathered], preferred_element_type=f32)
    out[:, gathered] = total.astype(bf16)
    for n in range(PARTS):
        cols = slice(width - apart + n * each, width - apart + (n + 1) * each)
        sums[n].wait_recv()
        out[:, cols] = (part[:, cols] + r_far[n].astype(f32)).astype(bf16)

    for cp in [near, w_near, w_far, w_fwd, ex_pair, ex_far, ex_skew, ex_near] + far + fwd + sums:
        cp.wait_send()
    for which in range(1 + GROUPS):

        @pl.when(c == 0)
        def _(which=which):
            across(sp, which).wait_send()

        @pl.loop(0, last_row - r)
        def _(i, which=which):
            along(sp, which, last_row - i).wait_send()

        @pl.loop(1, r + 1)
        def _(i, which=which):
            across(sp - 2 * i, which).wait_send()


def per_device(sp_size, tokens, w_query, w_key, w_value, w_out, cum_gate):
    rows, width = tokens.shape
    half, block = 2 * rows, 4 * rows
    heads = w_query.shape[1] // HD
    out_width = w_out.shape[1]
    extra = -(-(3 * heads + 3) // 16) * 16
    bf16, f32 = jnp.bfloat16, jnp.float32
    dma = pltpu.SemaphoreType.DMA
    anywhere = pl.BlockSpec(memory_space=pltpu.HBM)
    strip = pltpu.VMEM((PARTS, rows, out_width * 5 // 16), bf16)
    return pl.pallas_call(
        functools.partial(kernel, sp_size),
        out_shape=pltpu.VMEM((rows, out_width), bf16),
        in_specs=[anywhere] * 6,
        out_specs=pl.BlockSpec(memory_space=pltpu.VMEM),
        scratch_shapes=[
            pltpu.VMEM((2, GROUPS, 2, rows // GROUPS, width), bf16),
            pltpu.VMEM(w_query.shape, bf16),
            pltpu.VMEM((2 * HD, width), bf16),
            pltpu.VMEM(cum_gate.shape, f32),
            pltpu.VMEM((sp_size, 2 * extra + block, 2 * HD), bf16),
            pltpu.VMEM((sp_size, block, 2 * HD), bf16),
            pltpu.VMEM((2, 4 * HD, heads * half), bf16),
            pltpu.VMEM((2, 8, heads * half), f32),
            pltpu.VMEM((2, HD + 16, heads * half), f32),
            pltpu.VMEM((2, GROUPS, 2, rows // GROUPS, heads * HD), bf16),
            pltpu.VMEM((rows, out_width), f32),
            strip, strip,
            pltpu.VMEM((4,) + w_out.shape, bf16),
            pltpu.VMEM((4, GROUPS, rows // GROUPS, w_out.shape[0]), bf16),
            pltpu.VMEM((GROUPS, rows // GROUPS, w_out.shape[0]), bf16),
            dma((5 + GROUPS,)),
            dma((1,)), dma((1,)),
            dma((CHUNKS,)), dma((CHUNKS,)),
            dma((CHUNKS,)), dma((CHUNKS,)),
            dma((sp_size // 2, 1 + GROUPS)), dma((sp_size // 2, 1 + GROUPS)), dma((sp_size, 1 + GROUPS)),
            dma((PARTS,)), dma((PARTS,)),
            pltpu.SemaphoreType.REGULAR,
            dma((3,)), dma((3,)), dma((4,)), dma((4,)),
        ],
        compiler_params=pltpu.CompilerParams(
            collective_id=0, has_side_effects=True, vmem_limit_bytes=62 * 1024 * 1024
        ),
    )(tokens, w_query, w_key.T, w_value.T, w_out, cum_gate)


def solution(mesh):
    placed = (
        P(("sp", "tp"), None),
        P(None, "tp"),
        P(None, "tp"),
        P(None, "tp"),
        P("tp", None),
        P("tp", "sp"),
    )
    return jax.shard_map(
        functools.partial(per_device, mesh.shape["sp"]),
        mesh=mesh, in_specs=placed, out_specs=P(("sp", "tp"), None), check_vma=False,
    )
```

time: 28.5 us -> 27.6 us (0.968)
  Pallas kernels: 27.3 us -> 26.7 us
    pallas_call x1, Pallas kernels: 27.3 us -> 26.7 us  [per_device(): pl.pallas_call(functools.partial(kernel, sp_size), out_shape=pltpu.VMEM((...]
where the time goes in v3:
time: 27.6 us; the launch traced here: 27.4 us
  Pallas kernels  26.7 us (97%)
  local copies, waits for them, and re-layouts  0.71 us (3%)
    pallas_call x1, Pallas kernels, per_device(): pl.pallas_call(functools.partial(kernel, sp_size), out_shape=pltpu.VMEM((...  26.7 us
    unnamed x1, local copies, waits for them, and re-layouts  0.71 us

profile of v3, /device:TPU:25, one launch (start us, length us, event | category | flops | bytes accessed | tf_op | source)
XLA Modules:
  0.0 27.4 jit_solution(16678255631642540937)
XLA Ops:
  0.0 26.7 %shard_map.64 = bf16[64,2048]{1,0:T(8,128)(2,1)S(1)} custom-call(bf16[64,2048]{1,0:T(8,128)(2,1)} %tok.1, bf16[2048,256]{1,0:T(8,128)(2,1)} %wq.1, bf16[64,2048]{1,0:T(8,128)(2,1)} %bitcast.2, bf16[64,2048]{1,0:T(8,128)(2,1)} %bitcast.3, bf16[256,2048]{1,0:T(8,128)(2,1)} %wo.1, f32[4,256]{1,0:T(4,128)} %gate.1), custom_call_target="tpu_custom_call" | custom-call | tf_op jit(solution)/shard_map/pallas_call | solution.py:441
  26.7 0.7 %copy.8 = bf16[64,2048]{1,0:T(8,128)(2,1)} copy(bf16[64,2048]{1,0:T(8,128)(2,1)S(1)} %shard_map.64) | data formatting | bytes 524288

commit v4 on v3

--- a/solution.py
+++ b/solution.py
@@ -11,7 +11,7 @@
 MESH = pl.DeviceIdType.MESH
 CHUNKS = 4
 GROUPS = 2
-PARTS = 2
+PARTS = 3
 FAR = -1e30
 
 
@@ -274,9 +274,6 @@
     send_own(0)
     loads[3].wait()
     project_q(0)
-    loads[4].wait()
-    w_near = remote(wg.at[t], wg.at[t], w_s.at[0], w_r.at[0], tp=t1)
-    w_near.start()
     unpack(sp)
     absorb((0, [(sp, *first_part)]), first=(0,))
     fwd = [forward(0), forward(1)]
@@ -288,13 +285,14 @@
         absorb((0, [(spx, *first_part)]))
 
     relay(0)
+    loads[4].wait()
+    w_far = remote(wg.at[t, :, gathered], wg.at[t, :, gathered], w_s.at[1], w_r.at[1], tp=t2)
+    w_far.start()
     fwd[0].wait_recv()
     fwd[1].wait_recv()
     project_kv(1)
     send_own(1)
     fwd.append(forward(2))
-    w_far = remote(wg.at[t, :, gathered], wg.at[t, :, gathered], w_s.at[1], w_r.at[1], tp=t2)
-    w_far.start()
 
     def directs(ids):
         srcs = [sp - 2 * i for i in ids]
@@ -342,6 +340,8 @@
         absorb((1, [(spx, *late)]), (0, [(spx, *late)]))
 
     relay(2)
+    w_near = remote(wg.at[t], wg.at[t], w_s.at[0], w_r.at[0], tp=t1)
+    w_near.start()
 
     def nearly(ids):
         near_by, beyond = [sp - 2 * i for i in ids], [spx - 2 * i for i in ids]
@@ -373,19 +373,21 @@
     ex_far.start()
     ex_skew = remote(others, ag.at[t], a_s.at[2], a_r.at[2], tp=t3)
     ex_skew.start()
-    over(lambda ids: absorb((0, [(spx - 2 * i, *late) for i in ids])))
 
     def flat(value):
         return value.reshape(rows, value.shape[-1])
 
+    each = s_far.shape[2]
+
+    strips = [slice(width - apart + n * each, width - apart + (n + 1) * each) for n in range(PARTS)]
+    for cols in strips:
+        part[:, cols] = jnp.dot(flat(att[1, :, core]), wg[t, :, cols], preferred_element_type=f32)
+    over(lambda ids: absorb((0, [(spx - 2 * i, *late) for i in ids])))
     w_near.wait_recv()
     ex_pair.wait_recv()
     sums = []
-    each = s_far.shape[2]
-    for n in range(PARTS):
-        cols = slice(width - apart + n * each, width - apart + (n + 1) * each)
-        both = jnp.dot(flat(att[1, :, core]), wg[t, :, cols], preferred_element_type=f32)
-        both += jnp.dot(flat(ae[...]), wg[t1, :, cols], preferred_element_type=f32)
+    for n, cols in enumerate(strips):
+        both = part[:, cols] + jnp.dot(flat(ae[...]), wg[t1, :, cols], preferred_element_type=f32)
         s_far[n] = both.astype(bf16)
         cp = remote(s_far.at[n], r_far.at[n], o_s.at[n], o_r.at[n], tp=t2)
         cp.start()
@@ -437,7 +439,7 @@
     bf16, f32 = jnp.bfloat16, jnp.float32
     dma = pltpu.SemaphoreType.DMA
     anywhere = pl.BlockSpec(memory_space=pltpu.HBM)
-    strip = pltpu.VMEM((PARTS, rows, out_width * 5 // 16), bf16)
+    strip = pltpu.VMEM((PARTS, rows, out_width * 3 // 16), bf16)
     return pl.pallas_call(
         functools.partial(kernel, sp_size),
         out_shape=pltpu.VMEM((rows, out_width), bf16),

time: 27.6 us -> 27.1 us (0.982)
  Pallas kernels: 26.7 us -> 26.3 us
    pallas_call x1, Pallas kernels: 26.7 us -> 26.3 us  [per_device(): pl.pallas_call(functools.partial(kernel, sp_size), out_shape=pltpu.VMEM((...]
where the time goes in v4:
time: 27.1 us; the launch traced here: 27 us
  Pallas kernels  26.3 us (97%)
  local copies, waits for them, and re-layouts  0.71 us (3%)
    pallas_call x1, Pallas kernels, per_device(): pl.pallas_call(functools.partial(kernel, sp_size), out_shape=pltpu.VMEM((...  26.3 us
    unnamed x1, local copies, waits for them, and re-layouts  0.71 us

profile of v4, /device:TPU:25, one launch (start us, length us, event | category | flops | bytes accessed | tf_op | source)
XLA Modules:
  0.0 27.0 jit_solution(7014447626471662915)
XLA Ops:
  0.0 26.3 %shard_map.64 = bf16[64,2048]{1,0:T(8,128)(2,1)S(1)} custom-call(bf16[64,2048]{1,0:T(8,128)(2,1)} %tok.1, bf16[2048,256]{1,0:T(8,128)(2,1)} %wq.1, bf16[64,2048]{1,0:T(8,128)(2,1)} %bitcast.2, bf16[64,2048]{1,0:T(8,128)(2,1)} %bitcast.3, bf16[256,2048]{1,0:T(8,128)(2,1)} %wo.1, f32[4,256]{1,0:T(4,128)} %gate.1), custom_call_target="tpu_custom_call" | custom-call | tf_op jit(solution)/shard_map/pallas_call | solution.py:443
  26.3 0.7 %copy.8 = bf16[64,2048]{1,0:T(8,128)(2,1)} copy(bf16[64,2048]{1,0:T(8,128)(2,1)S(1)} %shard_map.64) | data formatting | bytes 524288

commit v5 on v4

--- a/solution.py
+++ b/solution.py
@@ -11,7 +11,7 @@
 MESH = pl.DeviceIdType.MESH
 CHUNKS = 4
 GROUPS = 2
-PARTS = 3
+SHARED = 4
 FAR = -1e30
 
 
@@ -20,7 +20,7 @@
     x, wqv, wboth, gv, kv, gk, qt, top, acc, att, part,
     s_far, r_far, wg, ag, ae,
     load, tok_s, tok_r, far_s, far_r, fwd_s, fwd_r,
-    z_s, x_s, kv_r, o_s, o_r, ready, w_s, w_r, a_s, a_r,
+    z_s, x_s, kv_r, o_s, o_r, ready, w_s, w_r, a_s, a_r, y_s, y_r, b_s, b_r, d_s, d_r,
 ):
     f32, bf16 = jnp.float32, jnp.bfloat16
     rows = tok.shape[0]
@@ -28,8 +28,10 @@
     block = 2 * half
     heads = wq.shape[1] // HD
     width = wo.shape[1]
-    apart = s_far.shape[0] * s_far.shape[2]
+    apart = s_far.shape[1]
     gathered = pl.ds(0, width - apart)
+    unit = width // 16
+    alone = pl.ds(2 * SHARED * unit, width - apart - 2 * SHARED * unit)
     sp = lax.axis_index("sp")
     t = lax.axis_index("tp")
     core = lax.rem(t, 2)
@@ -93,11 +95,11 @@
             device_id=where, device_id_type=MESH,
         )
 
-    far = []
-    for n in range(CHUNKS):
-        cp = remote(piece(0, n), piece(1, n), far_s.at[n], far_r.at[n], tp=t2)
+    far = [
+        remote(piece(0, n), piece(1, n), far_s.at[n], far_r.at[n], tp=t2) for n in range(CHUNKS)
+    ]
+    for cp in far[: CHUNKS // GROUPS]:
         cp.start()
-        far.append(cp)
     mine = x.at[0, :, core]
     near = remote(mine, mine, tok_s.at[0], tok_r.at[0], tp=t1)
     near.start()
@@ -248,6 +250,26 @@
         def _():
             work([r - 1, r])
 
+    def strip(k, side):
+        return pl.ds(pl.multiple_of((side * SHARED + k) * unit, unit), unit)
+
+    def over_x(k, side):
+        ref = wg.at[t2, :, strip(k, side)]
+        return remote(ref, ref, b_s.at[k], b_r.at[k], sp=spx)
+
+    def over_chip(k, side, n):
+        ref = wg.at[t2, :, strip(k, side)]
+        return remote(ref, ref, d_s.at[n, k], d_r.at[n, k], tp=t1)
+
+    def share(k):
+        c_far[k].wait_recv()
+        over_x(k, c).start()
+        over_chip(k, c, 0).start()
+
+    def pass_on(k):
+        over_x(k, 1 - c).wait_recv()
+        over_chip(k, 1 - c, 1).start()
+
     def forward(n):
         far[n].wait_recv()
         cp = remote(piece(1, n), piece(1, n), fwd_s.at[n], fwd_r.at[n], tp=t1)
@@ -265,6 +287,12 @@
     loads[1].wait()
     loads[2].wait()
     near.wait_recv()
+
+    @pl.when(core == 0)
+    def _():
+        for cp in far[CHUNKS // GROUPS :]:
+            cp.start()
+
     project_kv(0)
 
     @pl.when(r == 0)
@@ -274,6 +302,12 @@
     send_own(0)
     loads[3].wait()
     project_q(0)
+
+    @pl.when(core == 1)
+    def _():
+        for cp in far[CHUNKS // GROUPS :]:
+            cp.start()
+
     unpack(sp)
     absorb((0, [(sp, *first_part)]), first=(0,))
     fwd = [forward(0), forward(1)]
@@ -286,7 +320,11 @@
 
     relay(0)
     loads[4].wait()
-    w_far = remote(wg.at[t, :, gathered], wg.at[t, :, gathered], w_s.at[1], w_r.at[1], tp=t2)
+    c_far, w_far = [], remote(wg.at[t, :, alone], wg.at[t, :, alone], w_s.at[1], w_r.at[1], tp=t2)
+    for k in range(SHARED):
+        ref = wg.at[t, :, strip(k, c)]
+        c_far.append(remote(ref, ref, y_s.at[k], y_r.at[k], tp=t2))
+        c_far[k].start()
     w_far.start()
     fwd[0].wait_recv()
     fwd[1].wait_recv()
@@ -309,6 +347,7 @@
     send_own(2)
     project_q(1)
     relay(1)
+    share(0)
 
     @pl.when(c == 0)
     def _():
@@ -334,14 +373,15 @@
 
     over(mixed)
 
-    @pl.when(c == 1)
-    def _():
-        across(spx, 2).wait_recv()
-        absorb((1, [(spx, *late)]), (0, [(spx, *late)]))
-
     relay(2)
     w_near = remote(wg.at[t], wg.at[t], w_s.at[0], w_r.at[0], tp=t1)
     w_near.start()
+    share(1)
+
+    @pl.when(c == 1)
+    def _():
+        across(spx, 2).wait_recv()
+        absorb((1, [(spx, *late)]), (0, [(spx, *late)]))
 
     def nearly(ids):
         near_by, beyond = [sp - 2 * i for i in ids], [spx - 2 * i for i in ids]
@@ -351,6 +391,8 @@
         absorb((1, pieces), (0, pieces))
 
     over(nearly)
+    for k in range(2, SHARED):
+        share(k)
 
     def lasts(ids):
         beyond = [spx - 2 * i for i in ids]
@@ -377,43 +419,54 @@
     def flat(value):
         return value.reshape(rows, value.shape[-1])
 
-    each = s_far.shape[2]
-
-    strips = [slice(width - apart + n * each, width - apart + (n + 1) * each) for n in range(PARTS)]
-    for cols in strips:
-        part[:, cols] = jnp.dot(flat(att[1, :, core]), wg[t, :, cols], preferred_element_type=f32)
+    middle = apart // 256 * 128
+    strips = (slice(0, middle), slice(middle, apart))
+    rest = slice(width - apart, width)
+    part[:, rest] = jnp.dot(flat(att[1, :, core]), wg[t, :, rest], preferred_element_type=f32)
     over(lambda ids: absorb((0, [(spx - 2 * i, *late) for i in ids])))
     w_near.wait_recv()
     ex_pair.wait_recv()
     sums = []
-    for n, cols in enumerate(strips):
+    for n, cut in enumerate(strips):
+        cols = slice(width - apart + cut.start, width - apart + cut.stop)
         both = part[:, cols] + jnp.dot(flat(ae[...]), wg[t1, :, cols], preferred_element_type=f32)
-        s_far[n] = both.astype(bf16)
-        cp = remote(s_far.at[n], r_far.at[n], o_s.at[n], o_r.at[n], tp=t2)
+        s_far[:, cut] = both.astype(bf16)
+        cp = remote(s_far.at[:, cut], r_far.at[:, cut], o_s.at[n], o_r.at[n], tp=t2)
         cp.start()
         sums.append(cp)
 
     settle(0)
+    for k in range(2):
+        pass_on(k)
     ex_near = remote(att.at[0, :, 1 - core], ag.at[t], a_s.at[0], a_r.at[0], tp=t1)
     ex_near.start()
     w_far.wait_recv()
-    w_fwd = remote(wg.at[t2, :, gathered], wg.at[t2, :, gathered], w_s.at[2], w_r.at[2], tp=t1)
+    w_fwd = remote(wg.at[t2, :, alone], wg.at[t2, :, alone], w_s.at[2], w_r.at[2], tp=t1)
     w_fwd.start()
     part[...] = jnp.dot(flat(att[0, :, core]), wg[t], preferred_element_type=f32)
+    for k in range(2, SHARED):
+        pass_on(k)
     ex_near.wait_recv()
     part[...] += jnp.dot(flat(ag[t1]), wg[t1], preferred_element_type=f32)
     ex_far.wait_recv()
     total = part[:, gathered] + jnp.dot(flat(ag[t2]), wg[t2, :, gathered], preferred_element_type=f32)
     ex_skew.wait_recv()
     w_fwd.wait_recv()
+    for k in range(SHARED):
+        over_chip(k, c, 0).wait_recv()
+        over_chip(k, 1 - c, 1).wait_recv()
     total = total + jnp.dot(flat(ag[t3]), wg[t3, :, gathered], preferred_element_type=f32)
     out[:, gathered] = total.astype(bf16)
-    for n in range(PARTS):
-        cols = slice(width - apart + n * each, width - apart + (n + 1) * each)
+    for n, cut in enumerate(strips):
+        cols = slice(width - apart + cut.start, width - apart + cut.stop)
         sums[n].wait_recv()
-        out[:, cols] = (part[:, cols] + r_far[n].astype(f32)).astype(bf16)
-
-    for cp in [near, w_near, w_far, w_fwd, ex_pair, ex_far, ex_skew, ex_near] + far + fwd + sums:
+        out[:, cols] = (part[:, cols] + r_far[:, cut].astype(f32)).astype(bf16)
+
+    for k in range(SHARED):
+        over_x(k, c).wait_send()
+        over_chip(k, c, 0).wait_send()
+        over_chip(k, 1 - c, 1).wait_send()
+    for cp in c_far + [near, w_near, w_far, w_fwd, ex_pair, ex_far, ex_skew, ex_near] + far + fwd + sums:
         cp.wait_send()
     for which in range(1 + GROUPS):
 
@@ -439,7 +492,7 @@
     bf16, f32 = jnp.bfloat16, jnp.float32
     dma = pltpu.SemaphoreType.DMA
     anywhere = pl.BlockSpec(memory_space=pltpu.HBM)
-    strip = pltpu.VMEM((PARTS, rows, out_width * 3 // 16), bf16)
+    summed = pltpu.VMEM((rows, out_width * 5 // 16), bf16)
     return pl.pallas_call(
         functools.partial(kernel, sp_size),
         out_shape=pltpu.VMEM((rows, out_width), bf16),
@@ -457,7 +510,7 @@
             pltpu.VMEM((2, HD + 16, heads * half), f32),
             pltpu.VMEM((2, GROUPS, 2, rows // GROUPS, heads * HD), bf16),
             pltpu.VMEM((rows, out_width), f32),
-            strip, strip,
+            summed, summed,
             pltpu.VMEM((4,) + w_out.shape, bf16),
             pltpu.VMEM((4, GROUPS, rows // GROUPS, w_out.shape[0]), bf16),
             pltpu.VMEM((GROUPS, rows // GROUPS, w_out.shape[0]), bf16),
@@ -466,9 +519,10 @@
             dma((CHUNKS,)), dma((CHUNKS,)),
             dma((CHUNKS,)), dma((CHUNKS,)),
             dma((sp_size // 2, 1 + GROUPS)), dma((sp_size // 2, 1 + GROUPS)), dma((sp_size, 1 + GROUPS)),
-            dma((PARTS,)), dma((PARTS,)),
+            dma((2,)), dma((2,)),
             pltpu.SemaphoreType.REGULAR,
             dma((3,)), dma((3,)), dma((4,)), dma((4,)),
+            dma((SHARED,)), dma((SHARED,)), dma((SHARED,)), dma((SHARED,)), dma((2, SHARED)), dma((2, SHARED)),
         ],
         compiler_params=pltpu.CompilerParams(
             collective_id=0, has_side_effects=True, vmem_limit_bytes=62 * 1024 * 1024

time: 27.1 us -> 26.1 us (0.963)
  Pallas kernels: 26.3 us -> 25.3 us
    pallas_call x1, Pallas kernels: 26.3 us -> 25.3 us  [per_device(): pl.pallas_call(functools.partial(kernel, sp_size), out_shape=pltpu.VMEM((...]
where the time goes in v5:
time: 26.1 us; the launch traced here: 26 us
  Pallas kernels  25.3 us (97%)
  local copies, waits for them, and re-layouts  0.71 us (3%)
    pallas_call x1, Pallas kernels, per_device(): pl.pallas_call(functools.partial(kernel, sp_size), out_shape=pltpu.VMEM((...  25.3 us
    unnamed x1, local copies, waits for them, and re-layouts  0.71 us

profile of v5, /device:TPU:25, one launch (start us, length us, event | category | flops | bytes accessed | tf_op | source)
XLA Modules:
  0.0 26.0 jit_solution(7317031902969638369)
XLA Ops:
  0.0 25.3 %shard_map.64 = bf16[64,2048]{1,0:T(8,128)(2,1)S(1)} custom-call(bf16[64,2048]{1,0:T(8,128)(2,1)} %tok.1, bf16[2048,256]{1,0:T(8,128)(2,1)} %wq.1, bf16[64,2048]{1,0:T(8,128)(2,1)} %bitcast.2, bf16[64,2048]{1,0:T(8,128)(2,1)} %bitcast.3, bf16[256,2048]{1,0:T(8,128)(2,1)} %wo.1, f32[4,256]{1,0:T(4,128)} %gate.1), custom_call_target="tpu_custom_call" | custom-call | tf_op jit(solution)/shard_map/pallas_call | solution.py:496
  25.3 0.7 %copy.8 = bf16[64,2048]{1,0:T(8,128)(2,1)} copy(bf16[64,2048]{1,0:T(8,128)(2,1)S(1)} %shard_map.64) | data formatting | bytes 524288

commit v6 on v5

--- a/solution.py
+++ b/solution.py
@@ -17,7 +17,7 @@
 
 def kernel(
     sp_size, tok, wq, wk, wv, wo, gate, out,
-    x, wqv, wboth, gv, kv, gk, qt, top, acc, att, part,
+    x, wqv, wboth, wt, gv, kv, gk, qt, top, acc, att, part,
     s_far, r_far, wg, ag, ae,
     load, tok_s, tok_r, far_s, far_r, fwd_s, fwd_r,
     z_s, x_s, kv_r, o_s, o_r, ready, w_s, w_r, a_s, a_r, y_s, y_r, b_s, b_r, d_s, d_r,
@@ -81,6 +81,9 @@
 
     for copy in arrive:
         copy.wait()
+    loads[1].wait()
+    loads[2].wait()
+    wt[...] = wboth[...].T
     peers = 4 + jnp.where(has_next, 1, 0) + jnp.where(r > 0, 1, 0)
     pl.semaphore_wait(barrier, peers)
 
@@ -144,10 +147,7 @@
     def project_kv(part_n):
         lo, hi_row = bounds[part_n], bounds[part_n + 1]
         xs = x[0] if part_n == 0 else x[1, part_n - 1]
-        both = lax.dot_general(
-            xs.reshape(hi_row - lo, x.shape[-1]), wboth[...], (((1,), (1,)), ((), ())),
-            preferred_element_type=f32,
-        )
+        both = jnp.dot(xs.reshape(hi_row - lo, x.shape[-1]), wt[...], preferred_element_type=f32)
         kv[sp, lead + lo : lead + hi_row, :] = both.astype(bf16)
 
     def project_q(kind):
@@ -284,8 +284,6 @@
 
     first_part, early, late, other = [(0, half), (half, bounds[2]), (bounds[2], block), (half, block)]
 
-    loads[1].wait()
-    loads[2].wait()
     near.wait_recv()
 
     @pl.when(core == 0)
@@ -361,22 +359,28 @@
             (0, [(sp, *late), (spx, *early)]), first=(1,),
         )
 
-    def mixed(ids):
-        near_by, beyond = [sp - 2 * i for i in ids], [spx - 2 * i for i in ids]
-        for src in beyond:
-            across(src, 0).wait_recv()
-            unpack(src)
+    def closer(ids):
+        near_by = [sp - 2 * i for i in ids]
         absorb(
-            (1, [(src, 0, bounds[2]) for src in near_by] + [(src, *first_part) for src in beyond]),
-            (0, [(src, *early) for src in near_by] + [(src, *first_part) for src in beyond]),
+            (1, [(src, 0, bounds[2]) for src in near_by]),
+            (0, [(src, *early) for src in near_by]),
         )
 
-    over(mixed)
-
+    over(closer)
     relay(2)
     w_near = remote(wg.at[t], wg.at[t], w_s.at[0], w_r.at[0], tp=t1)
     w_near.start()
     share(1)
+
+    def beyond_x(ids):
+        beyond = [spx - 2 * i for i in ids]
+        for src in beyond:
+            across(src, 0).wait_recv()
+            unpack(src)
+        pieces = [(src, *first_part) for src in beyond]
+        absorb((1, pieces), (0, pieces))
+
+    over(beyond_x)
 
     @pl.when(c == 1)
     def _():
@@ -502,6 +506,7 @@
             pltpu.VMEM((2, GROUPS, 2, rows // GROUPS, width), bf16),
             pltpu.VMEM(w_query.shape, bf16),
             pltpu.VMEM((2 * HD, width), bf16),
+            pltpu.VMEM((width, 2 * HD), bf16),
             pltpu.VMEM(cum_gate.shape, f32),
             pltpu.VMEM((sp_size, 2 * extra + block, 2 * HD), bf16),
             pltpu.VMEM((sp_size, block, 2 * HD), bf16),

time: 26.1 us -> 25.7 us (0.985)
  Pallas kernels: 25.3 us -> 24.8 us
    pallas_call x1, Pallas kernels: 25.3 us -> 24.8 us  [per_device(): pl.pallas_call(functools.partial(kernel, sp_size), out_shape=pltpu.VMEM((...]
where the time goes in v6:
time: 25.7 us; the launch traced here: 25.6 us
  Pallas kernels  24.8 us (96%)
  local copies, waits for them, and re-layouts  0.71 us (3%)
    pallas_call x1, Pallas kernels, per_device(): pl.pallas_call(functools.partial(kernel, sp_size), out_shape=pltpu.VMEM((...  24.8 us
    unnamed x1, local copies, waits for them, and re-layouts  0.71 us

profile of v6, /device:TPU:25, one launch (start us, length us, event | category | flops | bytes accessed | tf_op | source)
XLA Modules:
  0.0 25.6 jit_solution(8621642854937140965)
XLA Ops:
  0.0 24.8 %shard_map.64 = bf16[64,2048]{1,0:T(8,128)(2,1)S(1)} custom-call(bf16[64,2048]{1,0:T(8,128)(2,1)} %tok.1, bf16[2048,256]{1,0:T(8,128)(2,1)} %wq.1, bf16[64,2048]{1,0:T(8,128)(2,1)} %bitcast.2, bf16[64,2048]{1,0:T(8,128)(2,1)} %bitcast.3, bf16[256,2048]{1,0:T(8,128)(2,1)} %wo.1, f32[4,256]{1,0:T(4,128)} %gate.1), custom_call_target="tpu_custom_call" | custom-call | tf_op jit(solution)/shard_map/pallas_call | solution.py:500
  24.9 0.7 %copy.8 = bf16[64,2048]{1,0:T(8,128)(2,1)} copy(bf16[64,2048]{1,0:T(8,128)(2,1)S(1)} %shard_map.64) | data formatting | bytes 524288

commit v7 on v6

--- a/solution.py
+++ b/solution.py
@@ -19,8 +19,7 @@
     sp_size, tok, wq, wk, wv, wo, gate, out,
     x, wqv, wboth, wt, gv, kv, gk, qt, top, acc, att, part,
     s_far, r_far, wg, ag, ae,
-    load, tok_s, tok_r, far_s, far_r, fwd_s, fwd_r,
-    z_s, x_s, kv_r, o_s, o_r, ready, w_s, w_r, a_s, a_r, y_s, y_r, b_s, b_r, d_s, d_r,
+    load, sent, tok_r, far_r, fwd_r, kv_r, o_r, ready, w_r, a_r, y_r, b_r, d_r,
 ):
     f32, bf16 = jnp.float32, jnp.bfloat16
     rows = tok.shape[0]
@@ -28,7 +27,7 @@
     block = 2 * half
     heads = wq.shape[1] // HD
     width = wo.shape[1]
-    apart = s_far.shape[1]
+    apart = r_far.shape[1]
     gathered = pl.ds(0, width - apart)
     unit = width // 16
     alone = pl.ds(2 * SHARED * unit, width - apart - 2 * SHARED * unit)
@@ -52,12 +51,12 @@
     loads = [
         pltpu.make_async_copy(gate, gv, load.at[0]),
         pltpu.make_async_copy(wk, wboth.at[0:HD], load.at[1]),
-        pltpu.make_async_copy(wv, wboth.at[HD : 2 * HD], load.at[2]),
-        pltpu.make_async_copy(wq, wqv, load.at[3]),
-        pltpu.make_async_copy(wo, wg.at[t], load.at[4]),
+        pltpu.make_async_copy(wv, wboth.at[HD : 2 * HD], load.at[1]),
+        pltpu.make_async_copy(wq, wqv, load.at[2]),
+        pltpu.make_async_copy(wo, wg.at[t], load.at[3]),
     ]
     arrive = [
-        pltpu.make_async_copy(tok.at[pl.ds(n * span, span)], x.at[0, n, core], load.at[5 + n])
+        pltpu.make_async_copy(tok.at[pl.ds(n * span, span)], x.at[0, n, core], load.at[4])
         for n in range(GROUPS)
     ]
     for copy in arrive:
@@ -65,6 +64,9 @@
     for copy in loads:
         copy.start()
 
+    def drain(ref, semaphore):
+        pltpu.make_async_copy(ref, ref, semaphore).wait()
+
     barrier = pltpu.get_barrier_semaphore()
     pl.semaphore_signal(barrier, inc=1, device_id={"tp": t1}, device_id_type=MESH)
     pl.semaphore_signal(barrier, inc=1, device_id={"tp": t2}, device_id_type=MESH)
@@ -79,10 +81,8 @@
     def _():
         pl.semaphore_signal(barrier, inc=1, device_id={"sp": sp - 2}, device_id_type=MESH)
 
-    for copy in arrive:
-        copy.wait()
-    loads[1].wait()
-    loads[2].wait()
+    drain(x.at[0, :, core], load.at[4])
+    drain(wboth, load.at[1])
     wt[...] = wboth[...].T
     peers = 4 + jnp.where(has_next, 1, 0) + jnp.where(r > 0, 1, 0)
     pl.semaphore_wait(barrier, peers)
@@ -99,12 +99,12 @@
         )
 
     far = [
-        remote(piece(0, n), piece(1, n), far_s.at[n], far_r.at[n], tp=t2) for n in range(CHUNKS)
+        remote(piece(0, n), piece(1, n), sent.at[0], far_r.at[n], tp=t2) for n in range(CHUNKS)
     ]
     for cp in far[: CHUNKS // GROUPS]:
         cp.start()
     mine = x.at[0, :, core]
-    near = remote(mine, mine, tok_s.at[0], tok_r.at[0], tp=t1)
+    near = remote(mine, mine, sent.at[0], tok_r.at[0], tp=t1)
     near.start()
 
     def place(n):
@@ -162,11 +162,11 @@
 
     def along(src, n, row):
         ref = message(src, n)
-        return remote(ref, ref, z_s.at[row, n], kv_r.at[src, n], sp=2 * row + c)
+        return remote(ref, ref, sent.at[1], kv_r.at[src, n], sp=2 * row + c)
 
     def across(src, n):
         ref = message(src, n)
-        return remote(ref, ref, x_s.at[src // 2, n], kv_r.at[src, n], sp=spx)
+        return remote(ref, ref, sent.at[1], kv_r.at[src, n], sp=spx)
 
     def send_own(n):
         @pl.loop(0, last_row - r)
@@ -255,11 +255,11 @@
 
     def over_x(k, side):
         ref = wg.at[t2, :, strip(k, side)]
-        return remote(ref, ref, b_s.at[k], b_r.at[k], sp=spx)
+        return remote(ref, ref, sent.at[2], b_r.at[k], sp=spx)
 
     def over_chip(k, side, n):
         ref = wg.at[t2, :, strip(k, side)]
-        return remote(ref, ref, d_s.at[n, k], d_r.at[n, k], tp=t1)
+        return remote(ref, ref, sent.at[2], d_r, tp=t1)
 
     def share(k):
         c_far[k].wait_recv()
@@ -272,7 +272,7 @@
 
     def forward(n):
         far[n].wait_recv()
-        cp = remote(piece(1, n), piece(1, n), fwd_s.at[n], fwd_r.at[n], tp=t1)
+        cp = remote(piece(1, n), piece(1, n), sent.at[0], fwd_r.at[n * step // span], tp=t1)
         cp.start()
         return cp
 
@@ -318,14 +318,13 @@
 
     relay(0)
     loads[4].wait()
-    c_far, w_far = [], remote(wg.at[t, :, alone], wg.at[t, :, alone], w_s.at[1], w_r.at[1], tp=t2)
+    c_far, w_far = [], remote(wg.at[t, :, alone], wg.at[t, :, alone], sent.at[4], w_r.at[1], tp=t2)
     for k in range(SHARED):
         ref = wg.at[t, :, strip(k, c)]
-        c_far.append(remote(ref, ref, y_s.at[k], y_r.at[k], tp=t2))
+        c_far.append(remote(ref, ref, sent.at[2], y_r.at[k], tp=t2))
         c_far[k].start()
     w_far.start()
-    fwd[0].wait_recv()
-    fwd[1].wait_recv()
+    drain(x.at[1, 0, 1 - core], fwd_r.at[0])
     project_kv(1)
     send_own(1)
     fwd.append(forward(2))
@@ -339,8 +338,7 @@
     over(directs)
     fwd.append(forward(3))
     absorb((0, [(sp, *early)]))
-    fwd[2].wait_recv()
-    fwd[3].wait_recv()
+    drain(x.at[1, 1, 1 - core], fwd_r.at[1])
     project_kv(2)
     send_own(2)
     project_q(1)
@@ -368,7 +366,7 @@
 
     over(closer)
     relay(2)
-    w_near = remote(wg.at[t], wg.at[t], w_s.at[0], w_r.at[0], tp=t1)
+    w_near = remote(wg.at[t], wg.at[t], sent.at[3], w_r.at[0], tp=t1)
     w_near.start()
     share(1)
 
@@ -413,11 +411,9 @@
 
     settle(1)
     theirs, others = att.at[1, :, core], att.at[1, :, 1 - core]
-    ex_pair = remote(others, ae, a_s.at[3], a_r.at[3], tp=t1)
-    ex_pair.start()
-    ex_far = remote(theirs, ag.at[t], a_s.at[1], a_r.at[1], tp=t2)
+    ex_far = remote(theirs, ag.at[t], sent.at[5], a_r.at[1], tp=t2)
     ex_far.start()
-    ex_skew = remote(others, ag.at[t], a_s.at[2], a_r.at[2], tp=t3)
+    ex_skew = remote(others, ag.at[t], sent.at[5], a_r.at[2], tp=t3)
     ex_skew.start()
 
     def flat(value):
@@ -425,27 +421,39 @@
 
     middle = apart // 256 * 128
     strips = (slice(0, middle), slice(middle, apart))
-    rest = slice(width - apart, width)
-    part[:, rest] = jnp.dot(flat(att[1, :, core]), wg[t, :, rest], preferred_element_type=f32)
+    ex_pair = remote(att.at[1], ae, sent.at[6], a_r.at[3], tp=t1)
+
+    def sums(n, side):
+        to = t2 if side == 0 else t3
+        cut = strips[n]
+        return remote(s_far.at[side, :, cut], r_far.at[:, cut], sent.at[6], o_r.at[n], tp=to)
+
+    w_near.wait_recv()
+
+    @pl.when(core == 1)
+    def _():
+        ex_pair.start()
+
+    @pl.when(core == 0)
+    def _():
+        ex_pair.wait_recv()
+        for n, cut in enumerate(strips):
+            cols = slice(width - apart + cut.start, width - apart + cut.stop)
+            both = jnp.dot(att[1].reshape(half, -1), wg[t, :, cols], preferred_element_type=f32)
+            both = both + jnp.dot(ae[...].reshape(half, -1), wg[t1, :, cols], preferred_element_type=f32)
+            both = both.astype(bf16).reshape(GROUPS, 2, span, -1)
+            for side in range(2):
+                s_far[side, :, cut] = both[:, side].reshape(rows, -1)
+                sums(n, side).start()
+
     over(lambda ids: absorb((0, [(spx - 2 * i, *late) for i in ids])))
-    w_near.wait_recv()
-    ex_pair.wait_recv()
-    sums = []
-    for n, cut in enumerate(strips):
-        cols = slice(width - apart + cut.start, width - apart + cut.stop)
-        both = part[:, cols] + jnp.dot(flat(ae[...]), wg[t1, :, cols], preferred_element_type=f32)
-        s_far[:, cut] = both.astype(bf16)
-        cp = remote(s_far.at[:, cut], r_far.at[:, cut], o_s.at[n], o_r.at[n], tp=t2)
-        cp.start()
-        sums.append(cp)
-
     settle(0)
     for k in range(2):
         pass_on(k)
-    ex_near = remote(att.at[0, :, 1 - core], ag.at[t], a_s.at[0], a_r.at[0], tp=t1)
+    ex_near = remote(att.at[0, :, 1 - core], ag.at[t], sent.at[5], a_r.at[0], tp=t1)
     ex_near.start()
     w_far.wait_recv()
-    w_fwd = remote(wg.at[t2, :, alone], wg.at[t2, :, alone], w_s.at[2], w_r.at[2], tp=t1)
+    w_fwd = remote(wg.at[t2, :, alone], wg.at[t2, :, alone], sent.at[4], w_r.at[2], tp=t1)
     w_fwd.start()
     part[...] = jnp.dot(flat(att[0, :, core]), wg[t], preferred_element_type=f32)
     for k in range(2, SHARED):
@@ -456,35 +464,36 @@
     total = part[:, gathered] + jnp.dot(flat(ag[t2]), wg[t2, :, gathered], preferred_element_type=f32)
     ex_skew.wait_recv()
     w_fwd.wait_recv()
-    for k in range(SHARED):
-        over_chip(k, c, 0).wait_recv()
-        over_chip(k, 1 - c, 1).wait_recv()
+    drain(wg.at[0, :, : 2 * SHARED * unit], d_r)
     total = total + jnp.dot(flat(ag[t3]), wg[t3, :, gathered], preferred_element_type=f32)
     out[:, gathered] = total.astype(bf16)
+    drain(wg.at[0:3, 0:rows], sent.at[0])
+
+    @pl.when(c == 0)
+    def _():
+        drain(kv.at[0 : last_row + 1], sent.at[1])
+
+    @pl.when(c == 1)
+    def _():
+        drain(kv.at[0:last_row], sent.at[1])
+
+    drain(wg.at[0, :, : 4 * SHARED * unit], sent.at[2])
+    w_near.wait_send()
+    drain(wg.at[0, :, : 2 * alone.size], sent.at[4])
+    drain(ag.at[0:3], sent.at[5])
+
     for n, cut in enumerate(strips):
         cols = slice(width - apart + cut.start, width - apart + cut.stop)
-        sums[n].wait_recv()
+        sums(n, 0).wait_recv()
         out[:, cols] = (part[:, cols] + r_far[:, cut].astype(f32)).astype(bf16)
 
-    for k in range(SHARED):
-        over_x(k, c).wait_send()
-        over_chip(k, c, 0).wait_send()
-        over_chip(k, 1 - c, 1).wait_send()
-    for cp in c_far + [near, w_near, w_far, w_fwd, ex_pair, ex_far, ex_skew, ex_near] + far + fwd + sums:
-        cp.wait_send()
-    for which in range(1 + GROUPS):
-
-        @pl.when(c == 0)
-        def _(which=which):
-            across(sp, which).wait_send()
-
-        @pl.loop(0, last_row - r)
-        def _(i, which=which):
-            along(sp, which, last_row - i).wait_send()
-
-        @pl.loop(1, r + 1)
-        def _(i, which=which):
-            across(sp - 2 * i, which).wait_send()
+    @pl.when(core == 1)
+    def _():
+        ex_pair.wait_send()
+
+    @pl.when(core == 0)
+    def _():
+        drain(s_far, sent.at[6])
 
 
 def per_device(sp_size, tokens, w_query, w_key, w_value, w_out, cum_gate):
@@ -496,7 +505,7 @@
     bf16, f32 = jnp.bfloat16, jnp.float32
     dma = pltpu.SemaphoreType.DMA
     anywhere = pl.BlockSpec(memory_space=pltpu.HBM)
-    summed = pltpu.VMEM((rows, out_width * 5 // 16), bf16)
+    summed = (rows, out_width * 5 // 16)
     return pl.pallas_call(
         functools.partial(kernel, sp_size),
         out_shape=pltpu.VMEM((rows, out_width), bf16),
@@ -515,19 +524,13 @@
             pltpu.VMEM((2, HD + 16, heads * half), f32),
             pltpu.VMEM((2, GROUPS, 2, rows // GROUPS, heads * HD), bf16),
             pltpu.VMEM((rows, out_width), f32),
-            summed, summed,
+            pltpu.VMEM((2,) + summed, bf16), pltpu.VMEM(summed, bf16),
             pltpu.VMEM((4,) + w_out.shape, bf16),
             pltpu.VMEM((4, GROUPS, rows // GROUPS, w_out.shape[0]), bf16),
-            pltpu.VMEM((GROUPS, rows // GROUPS, w_out.shape[0]), bf16),
-            dma((5 + GROUPS,)),
-            dma((1,)), dma((1,)),
-            dma((CHUNKS,)), dma((CHUNKS,)),
-            dma((CHUNKS,)), dma((CHUNKS,)),
-            dma((sp_size // 2, 1 + GROUPS)), dma((sp_size // 2, 1 + GROUPS)), dma((sp_size, 1 + GROUPS)),
-            dma((2,)), dma((2,)),
-            pltpu.SemaphoreType.REGULAR,
-            dma((3,)), dma((3,)), dma((4,)), dma((4,)),
-            dma((SHARED,)), dma((SHARED,)), dma((SHARED,)), dma((SHARED,)), dma((2, SHARED)), dma((2, SHARED)),
+            pltpu.VMEM((GROUPS, 2, rows // GROUPS, w_out.shape[0]), bf16),
+            dma((5,)), dma((7,)), dma((1,)), dma((CHUNKS,)), dma((GROUPS,)),
+            dma((sp_size, 1 + GROUPS)), dma((2,)), pltpu.SemaphoreType.REGULAR,
+            dma((3,)), dma((4,)), dma((SHARED,)), dma((SHARED,)), dma(()),
         ],
         compiler_params=pltpu.CompilerParams(
             collective_id=0, has_side_effects=True, vmem_limit_bytes=62 * 1024 * 1024

time: 25.7 us -> 24.8 us (0.965)
  Pallas kernels: 24.8 us -> 23.9 us
    pallas_call x1, Pallas kernels: 24.8 us -> 23.9 us  [per_device(): pl.pallas_call(functools.partial(kernel, sp_size), out_shape=pltpu.VMEM((...]
where the time goes in v7:
time: 24.8 us; the launch traced here: 24.6 us
  Pallas kernels  23.9 us (96%)
  local copies, waits for them, and re-layouts  0.71 us (3%)
    pallas_call x1, Pallas kernels, per_device(): pl.pallas_call(functools.partial(kernel, sp_size), out_shape=pltpu.VMEM((...  23.9 us
    unnamed x1, local copies, waits for them, and re-layouts  0.71 us

profile of v7, /device:TPU:25, one launch (start us, length us, event | category | flops | bytes accessed | tf_op | source)
XLA Modules:
  0.0 24.6 jit_solution(13268156765863984656)
XLA Ops:
  0.0 23.9 %shard_map.64 = bf16[64,2048]{1,0:T(8,128)(2,1)S(1)} custom-call(bf16[64,2048]{1,0:T(8,128)(2,1)} %tok.1, bf16[2048,256]{1,0:T(8,128)(2,1)} %wq.1, bf16[64,2048]{1,0:T(8,128)(2,1)} %bitcast.2, bf16[64,2048]{1,0:T(8,128)(2,1)} %bitcast.3, bf16[256,2048]{1,0:T(8,128)(2,1)} %wo.1, f32[4,256]{1,0:T(4,128)} %gate.1), custom_call_target="tpu_custom_call" | custom-call | tf_op jit(solution)/shard_map/pallas_call | solution.py:509
  23.9 0.7 %copy.8 = bf16[64,2048]{1,0:T(8,128)(2,1)} copy(bf16[64,2048]{1,0:T(8,128)(2,1)S(1)} %shard_map.64) | data formatting | bytes 524288

commit v8 on v7

--- a/solution.py
+++ b/solution.py
@@ -343,7 +343,10 @@
     send_own(2)
     project_q(1)
     relay(1)
-    share(0)
+
+    @pl.when(core == 1)
+    def _():
+        share(0)
 
     @pl.when(c == 0)
     def _():
@@ -368,6 +371,11 @@
     relay(2)
     w_near = remote(wg.at[t], wg.at[t], sent.at[3], w_r.at[0], tp=t1)
     w_near.start()
+
+    @pl.when(core == 0)
+    def _():
+        share(0)
+
     share(1)
 
     def beyond_x(ids):
@@ -505,7 +513,7 @@
     bf16, f32 = jnp.bfloat16, jnp.float32
     dma = pltpu.SemaphoreType.DMA
     anywhere = pl.BlockSpec(memory_space=pltpu.HBM)
-    summed = (rows, out_width * 5 // 16)
+    summed = (rows, out_width * 6 // 16)
     return pl.pallas_call(
         functools.partial(kernel, sp_size),
         out_shape=pltpu.VMEM((rows, out_width), bf16),

time: 24.8 us -> 24.8 us (level)
  no operation moved by 1% of the time
where the time goes in v8:
time: 24.8 us; the launch traced here: 24.6 us
  Pallas kernels  23.9 us (96%)
  local copies, waits for them, and re-layouts  0.71 us (3%)
    pallas_call x1, Pallas kernels, per_device(): pl.pallas_call(functools.partial(kernel, sp_size), out_shape=pltpu.VMEM((...  23.9 us
    unnamed x1, local copies, waits for them, and re-layouts  0.71 us

profile of v8, /device:TPU:25, one launch (start us, length us, event | category | flops | bytes accessed | tf_op | source)
XLA Modules:
  0.0 24.6 jit_solution(14007916090337301369)
XLA Ops:
  0.0 23.9 %shard_map.64 = bf16[64,2048]{1,0:T(8,128)(2,1)S(1)} custom-call(bf16[64,2048]{1,0:T(8,128)(2,1)} %tok.1, bf16[2048,256]{1,0:T(8,128)(2,1)} %wq.1, bf16[64,2048]{1,0:T(8,128)(2,1)} %bitcast.2, bf16[64,2048]{1,0:T(8,128)(2,1)} %bitcast.3, bf16[256,2048]{1,0:T(8,128)(2,1)} %wo.1, f32[4,256]{1,0:T(4,128)} %gate.1), custom_call_target="tpu_custom_call" | custom-call | tf_op jit(solution)/shard_map/pallas_call | solution.py:517
  23.9 0.7 %copy.8 = bf16[64,2048]{1,0:T(8,128)(2,1)} copy(bf16[64,2048]{1,0:T(8,128)(2,1)S(1)} %shard_map.64) | data formatting | bytes 524288

commit v9 on v8

--- a/solution.py
+++ b/solution.py
@@ -323,7 +323,6 @@
         ref = wg.at[t, :, strip(k, c)]
         c_far.append(remote(ref, ref, sent.at[2], y_r.at[k], tp=t2))
         c_far[k].start()
-    w_far.start()
     drain(x.at[1, 0, 1 - core], fwd_r.at[0])
     project_kv(1)
     send_own(1)
@@ -392,6 +391,8 @@
     def _():
         across(spx, 2).wait_recv()
         absorb((1, [(spx, *late)]), (0, [(spx, *late)]))
+
+    w_far.start()
 
     def nearly(ids):
         near_by, beyond = [sp - 2 * i for i in ids], [spx - 2 * i for i in ids]

time: 24.8 us -> 24.8 us (level)
  no operation moved by 1% of the time
where the time goes in v9:
time: 24.8 us; the launch traced here: 24.6 us
  Pallas kernels  23.9 us (96%)
  local copies, waits for them, and re-layouts  0.71 us (3%)
    pallas_call x1, Pallas kernels, per_device(): pl.pallas_call(functools.partial(kernel, sp_size), out_shape=pltpu.VMEM((...  23.9 us
    unnamed x1, local copies, waits for them, and re-layouts  0.71 us

profile of v9, /device:TPU:25, one launch (start us, length us, event | category | flops | bytes accessed | tf_op | source)
XLA Modules:
  0.0 24.6 jit_solution(2368633011529754846)
XLA Ops:
  0.0 23.9 %shard_map.64 = bf16[64,2048]{1,0:T(8,128)(2,1)S(1)} custom-call(bf16[64,2048]{1,0:T(8,128)(2,1)} %tok.1, bf16[2048,256]{1,0:T(8,128)(2,1)} %wq.1, bf16[64,2048]{1,0:T(8,128)(2,1)} %bitcast.2, bf16[64,2048]{1,0:T(8,128)(2,1)} %bitcast.3, bf16[256,2048]{1,0:T(8,128)(2,1)} %wo.1, f32[4,256]{1,0:T(4,128)} %gate.1), custom_call_target="tpu_custom_call" | custom-call | tf_op jit(solution)/shard_map/pallas_call | solution.py:518
  23.9 0.7 %copy.8 = bf16[64,2048]{1,0:T(8,128)(2,1)} copy(bf16[64,2048]{1,0:T(8,128)(2,1)S(1)} %shard_map.64) | data formatting | bytes 524288
